TPU v7x, 256 devices: a whole 4x4x8 slice. The times are simulated.
256 devices in a mesh: ep: 16 (over y, x), tp: 16 (over z, core).
Axes of the slice: x: 4, y: 4, z: 8, core: 2. Of those that a mesh axis runs over, the one named last changes fastest.
Arguments:
- tokens: bfloat16 [512, 4096], P('ep'), may hold values from -6 to 6
- state_matrix: float32 [512, 16, 128, 128], P('ep', 'tp'), may hold values from -1.5 to 1.5
- state_norm: float32 [512, 16, 128], P('ep', 'tp'), may hold values from -4 to 4
- state_max: float32 [512, 16], P('ep', 'tp'), may hold values from -5 to 5
- mixer_gain: float32 [4096], replicated, may hold values from 0.1 to 1.9
- w_query: bfloat16 [4096, 2048], P('ep', 'tp'), may hold values from -0.09375 to 0.09375
- w_key: bfloat16 [4096, 2048], P('ep', 'tp'), may hold values from -0.09375 to 0.09375
- w_value: bfloat16 [4096, 2048], P('ep', 'tp'), may hold values from -0.09375 to 0.09375
- w_outgate: bfloat16 [4096, 2048], P('ep', 'tp'), may hold values from -0.09375 to 0.09375
- w_ingate: bfloat16 [4096, 16], replicated, may hold values from -0.09375 to 0.09375
- w_forget: bfloat16 [4096, 16], replicated, may hold values from -0.09375 to 0.09375
- forget_bias: float32 [16], replicated, may hold values from -2 to 4
- w_proj: bfloat16 [2048, 4096], P('tp', 'ep'), may hold values from -0.125 to 0.125
- ffn_gain: float32 [4096], replicated, may hold values from 0.1 to 1.9
- w_branch: bfloat16 [4096], replicated, may hold values from -0.09375 to 0.09375
- routes: int32 [512, 2], P('ep'), may hold values from 0 to 15, all different within a row; in each aligned block of 32 rows (0 to 31, 32 to 63, ...) at most 6 rows name the same one
- route_weight: float32 [512, 2], P('ep'), may hold values from 0.2 to 1
- expert_gate: bfloat16 [16, 4096, 4096], P('ep', None, 'tp'), may hold values from -0.09375 to 0.09375
- expert_up: bfloat16 [16, 4096, 4096], P('ep', None, 'tp'), may hold values from -0.09375 to 0.09375
- expert_down: bfloat16 [16, 4096, 4096], P('ep', 'tp'), may hold values from -0.09375 to 0.09375
- dense_gate: bfloat16 [4096, 8192], P('ep', 'tp'), may hold values from -0.09375 to 0.09375
- dense_up: bfloat16 [4096, 8192], P('ep', 'tp'), may hold values from -0.09375 to 0.09375
- dense_down: bfloat16 [8192, 4096], P('tp', 'ep'), may hold values from -0.0625 to 0.0625
Outputs:
- layer_out: bfloat16 [512, 4096], P('ep')
- new_matrix: float32 [512, 16, 128, 128], P('ep', 'tp')
- new_norm: float32 [512, 16, 128], P('ep', 'tp')
- new_max: float32 [512, 16], P('ep', 'tp')
Inputs may be any that keep to these rules, and one draw needn't show every extreme that they name: `routes`: each row names 2 different experts. Among the rows of one index of ep (32 sequences) no expert is named more than 6 times, and in some such group one expert is named exactly 6 times.
All inputs are finite; a program needn't handle non-finite values.
Results may differ from a plain program's by a relative error of at most 0.012.
Values may be sent and summed in bfloat16 or wider, within the bound.
A program may use at most 64 MiB of HBM per device.

v0:
```python
import jax
import jax.numpy as jnp
from jax import lax
from jax.sharding import PartitionSpec as P

EPS = 1e-06


def side_by_side(arrays, axis, dim, along):
    ends, at = ([], 0)
    for a in arrays[:-1]:
        at += a.shape[along]
        ends.append(at)
    both = jnp.concatenate(arrays, axis=along)
    return tuple(jnp.split(lax.all_gather(both, axis, axis=dim, tiled=True), ends, axis=along))


def from_everyone(shard, axis):
    devices = lax.axis_size(axis)
    return lax.all_to_all(
        jnp.broadcast_to(shard[None], (devices, *shard.shape)), axis, 0, 0, tiled=True
    )


def laid_out(parts, dim):
    parts = jnp.moveaxis(parts, 0, dim)
    shape = parts.shape
    return parts.reshape(*shape[:dim], shape[dim] * shape[dim + 1], *shape[dim + 2 :])


def collect(shard, axis, dim):
    parts = from_everyone(shard, axis)
    return laid_out(parts, dim)


def total_of_pieces(shard, axis):
    return lax.all_gather(shard, axis).sum(0)


def in_blocks(shard, dim, devices):
    shape = shard.shape
    parts = shard.reshape(*shape[:dim], devices, shape[dim] // devices, *shape[dim + 1 :])
    return jnp.moveaxis(parts, dim, 0)


def sum_at_owner(shard, axis, dim):
    parts = in_blocks(shard, dim, lax.axis_size(axis))
    arrived = lax.all_to_all(parts, axis, split_axis=0, concat_axis=0, tiled=True)
    return arrived.astype(jnp.float32).sum(axis=0)


def in_one_piece(arrays, axis, dim, along):
    both = jnp.concatenate(arrays, axis=along)
    out, at, finished = (sum_at_owner(both, axis, dim), 0, [])
    for a in arrays:
        finished.append(lax.slice_in_dim(out, at, at + a.shape[along], axis=along))
        at += a.shape[along]
    return tuple(finished)


def rms_scale(values, gain):
    wide = values.astype(jnp.float32)
    return wide * lax.rsqrt(jnp.mean(wide * wide, axis=-1, keepdims=True) + EPS) * gain


def slot_numbers(flat_routes, experts_all):
    onehot = (flat_routes[:, None] == jnp.arange(experts_all, dtype=jnp.int32)[None, :]).astype(
        jnp.int32
    )
    before = jnp.cumsum(onehot, axis=0) - onehot
    return jnp.sum(before * onehot, axis=1)


def memory_step(
    query_all,
    key_all,
    value_all,
    outgate,
    gate_in,
    gate_forget,
    state_matrix,
    state_norm,
    state_max,
):
    row_count, head_count = gate_in.shape
    head_size = state_matrix.shape[-1]
    heads_q = query_all.reshape(row_count, head_count, head_size)
    heads_k = key_all.reshape(row_count, head_count, head_size) * head_size ** (-0.5)
    heads_v = value_all.reshape(row_count, head_count, head_size)
    log_keep = jax.nn.log_sigmoid(gate_forget)
    new_max = jnp.maximum(log_keep + state_max, gate_in)
    keep_factor = jnp.exp(log_keep + state_max - new_max)
    write_factor = jnp.exp(gate_in - new_max)
    new_matrix = (
        keep_factor[:, :, None, None] * state_matrix
        + write_factor[:, :, None, None] * heads_k[:, :, :, None] * heads_v[:, :, None, :]
    )
    new_norm = keep_factor[:, :, None] * state_norm + write_factor[:, :, None] * heads_k
    numer = jnp.einsum("bhk,bhkv->bhv", heads_q, new_matrix, precision=lax.Precision.HIGHEST)
    denom = jnp.sum(heads_q * new_norm, axis=-1)
    cell = numer / jnp.maximum(jnp.abs(denom), 1.0)[:, :, None]
    gated = jax.nn.sigmoid(outgate.reshape(row_count, head_count, head_size)) * cell
    mixed_heads = gated.reshape(row_count, head_count * head_size).astype(jnp.bfloat16)
    return (mixed_heads, new_matrix, new_norm, new_max)


def on_device(
    tokens,
    state_matrix,
    state_norm,
    state_max,
    mixer_gain,
    w_query,
    w_key,
    w_value,
    w_outgate,
    w_ingate,
    w_forget,
    forget_bias,
    w_proj,
    ffn_gain,
    w_branch,
    routes,
    route_weight,
    expert_gate,
    expert_up,
    expert_down,
    dense_gate,
    dense_up,
    dense_down,
):
    row_count = tokens.shape[0]
    head_count = state_matrix.shape[1]
    model_width = tokens.shape[1]
    normed = rms_scale(tokens, mixer_gain).astype(jnp.bfloat16)
    head_start = lax.axis_index("tp") * head_count
    gate_in = lax.dynamic_slice_in_dim(
        jnp.dot(normed, w_ingate, preferred_element_type=jnp.float32), head_start, head_count, 1
    )
    forget_all = jnp.dot(normed, w_forget, preferred_element_type=jnp.float32) + forget_bias
    gate_forget = lax.dynamic_slice_in_dim(forget_all, head_start, head_count, 1)
    pieces = side_by_side((w_query, w_key, w_value, w_outgate), "ep", 0, 1)
    projected = tuple(
        (jnp.dot(normed, shard_w, preferred_element_type=jnp.float32) for shard_w in pieces)
    )
    mixed_heads, new_matrix, new_norm, new_max = memory_step(
        projected[0],
        projected[1],
        projected[2],
        projected[3],
        gate_in,
        gate_forget,
        state_matrix,
        state_norm,
        state_max,
    )
    spread_out = jnp.dot(collect(mixed_heads, "ep", 0), w_proj, preferred_element_type=jnp.float32)
    mix_back = lax.all_to_all(spread_out, "ep", split_axis=0, concat_axis=1, tiled=True)
    mixer_out = total_of_pieces(mix_back, "tp")
    residual = (tokens.astype(jnp.float32) + mixer_out).astype(jnp.bfloat16)
    ffn_in = rms_scale(residual, ffn_gain).astype(jnp.bfloat16)
    branch_share = jax.nn.sigmoid(jnp.dot(ffn_in, w_branch, preferred_element_type=jnp.float32))
    dense_spread = lax.all_to_all(ffn_in, "ep", split_axis=1, concat_axis=0, tiled=True)
    dense_g, dense_u = in_one_piece(
        (
            jnp.dot(dense_spread, dense_gate, preferred_element_type=jnp.float32).astype(
                jnp.bfloat16
            ),
            jnp.dot(dense_spread, dense_up, preferred_element_type=jnp.float32).astype(
                jnp.bfloat16
            ),
        ),
        "ep",
        0,
        1,
    )
    dense_hidden = (jax.nn.silu(dense_g) * dense_u).astype(jnp.bfloat16)
    dense_spread_out = jnp.dot(
        collect(dense_hidden, "ep", 0), dense_down, preferred_element_type=jnp.float32
    )
    dense_back = lax.all_to_all(dense_spread_out, "ep", split_axis=0, concat_axis=1, tiled=True)
    ep_count = lax.axis_size("ep")
    local_experts = expert_gate.shape[0]
    experts_all = local_experts * ep_count
    top_count = routes.shape[1]
    capacity = max(2, (row_count * top_count * 4 + 3 * experts_all - 1) // (3 * experts_all))
    flat_routes = routes.reshape(-1)
    slots = slot_numbers(flat_routes, experts_all)
    outbound = (
        jnp.zeros((experts_all, capacity, model_width), jnp.bfloat16)
        .at[flat_routes, slots]
        .set(jnp.repeat(ffn_in, top_count, axis=0))
    )
    arrived = lax.all_to_all(outbound, "ep", split_axis=0, concat_axis=0, tiled=True)
    slot_count = arrived.shape[1]
    grid = arrived.reshape(ep_count, local_experts, slot_count, model_width)
    gate_part = jnp.einsum("secd,edf->secf", grid, expert_gate, preferred_element_type=jnp.float32)
    up_part = jnp.einsum("secd,edf->secf", grid, expert_up, preferred_element_type=jnp.float32)
    hidden = (jax.nn.silu(gate_part) * up_part).astype(jnp.bfloat16)
    partial_out = jnp.einsum(
        "secf,efd->secd", hidden, expert_down, preferred_element_type=jnp.float32
    )
    partial_out = sum_at_owner(partial_out.astype(jnp.bfloat16), "tp", 3)
    partial_out = partial_out.reshape(ep_count * local_experts, slot_count, partial_out.shape[3])
    returned = lax.all_to_all(
        partial_out.astype(jnp.bfloat16), "ep", split_axis=0, concat_axis=0, tiled=True
    ).astype(partial_out.dtype)
    picked = returned[flat_routes, slots].reshape(row_count, top_count, returned.shape[2])
    shares = route_weight / jnp.sum(route_weight, axis=1, keepdims=True)
    expert_rows = jnp.sum(shares[:, :, None] * picked, axis=1)
    dense_slice = sum_at_owner((branch_share[:, None] * dense_back).astype(jnp.bfloat16), "tp", 1)
    width_part = dense_slice.shape[1]
    resid_slice = lax.dynamic_slice_in_dim(
        residual, lax.axis_index("tp") * width_part, width_part, 1
    )
    out_slice = (resid_slice.astype(jnp.float32) + expert_rows + dense_slice).astype(jnp.bfloat16)
    layer_out = collect(out_slice, "tp", 1)
    return (layer_out, new_matrix, new_norm, new_max)


def solution(mesh):
    in_specs = (
        P("ep", None),
        P("ep", "tp", None, None),
        P("ep", "tp", None),
        P("ep", "tp"),
        P(),
        P("ep", "tp"),
        P("ep", "tp"),
        P("ep", "tp"),
        P("ep", "tp"),
        P(),
        P(),
        P(),
        P("tp", "ep"),
        P(),
        P(),
        P("ep", None),
        P("ep", None),
        P("ep", None, "tp"),
        P("ep", None, "tp"),
        P("ep", "tp", None),
        P("ep", "tp"),
        P("ep", "tp"),
        P("tp", "ep"),
    )
    out_specs = (P("ep", None), P("ep", "tp", None, None), P("ep", "tp", None), P("ep", "tp"))
    return jax.shard_map(
        on_device, mesh=mesh, in_specs=in_specs, out_specs=out_specs, check_vma=False
    )
```

profile of v0, /device:TPU:17, one launch (start us, length us, event | category | flops | bytes accessed | tf_op | source)
XLA Modules:
  0.0 335.4 jit_solution(3360213346436248407)
XLA Ops:
  7.3 1.8 pad_maximum_fusion.1
  9.2 1.2 dynamic-slice
  10.4 1.1 fusion.45
  11.5 1.3 fusion.72
  12.8 1.3 fusion.74
  14.1 0.7 exponential_bitcast_fusion
  14.8 55.3 %all-gather.3.cloned.1.call-done = bf16[4096,512]{1,0:T(8,128)(2,1)} async-done(((bf16[256,512]{1,0:T(8,128)(2,1)}), bf16[4096,512]{1,0:T(8,128)(2,1)}) %all-gather.3.cloned.1.call-update) | async-done | bytes 4194320 | tf_op jit(solution)/shard_map/all_gather | solution.py:15
  70.1 1.7 convolution_multiply_fusion
  71.8 2.2 fusion.61
  74.0 1.6 fusion.31
  75.6 0.8 multiply_add_fusion
  76.4 1.9 fusion.5
  78.2 1.6 fusion.26
  79.9 9.7 %all_to_all.82 = bf16[16,32,128]{2,1,0:T(8,128)(2,1)S(1)} all-to-all(bf16[16,32,128]{2,1,0:T(8,128)(2,1)S(1)} %broadcast_in_dim.10), channel_id=1, replica_groups=mesh['ep'=16,'tp'=16] {'ep'}, dimensions={0} | all-to-all | bytes 262144 | tf_op jit(solution)/shard_map/all_to_all | solution.py:20
  89.7 12.4 %all_to_all.83 = f32[16,32,256]{2,1,0:T(8,128)S(1)} all-to-all(f32[16,32,256]{2,1,0:T(8,128)S(1)} %fusion.57), channel_id=1, replica_groups=mesh['ep'=16,'tp'=16] {'ep'}, dimensions={0} | all-to-all | bytes 1048576 | tf_op jit(solution)/shard_map/all_to_all | solution.py:158
  102.5 0.9 all_gather.10
  103.5 58.5 %all-gather.5.cloned.1.call-done = f32[16,32,4096]{2,1,0:T(8,128)} async-done(((f32[1,32,4096]{2,1,0:T(8,128)}), f32[16,32,4096]{2,1,0:T(8,128)}) %all-gather.5.cloned.1.call-update) | async-done | bytes 8388624 | tf_op jit(solution)/shard_map/all_gather | solution.py:37
  162.0 3.8 %reduce_sum.97 = f32[32,4096]{1,0:T(8,128)S(1)} reduce(f32[16,32,4096]{2,1,0:T(8,128)} %all-gather.5.cloned.1.call-done, f32[]{:T(128)} %constant.13.clone.1), dimensions={0}, to_apply=%region_2.3 | reduce | flops 1966080 | bytes 8912900 | tf_op jit(solution)/shard_map/reduce_sum | solution.py:37
  166.2 12.4 %all_to_all.84 = bf16[32,16,256]{2,0,1:T(8,128)(2,1)S(1)} all-to-all(bf16[32,16,256]{2,0,1:T(8,128)(2,1)S(1)} %bitcast.138), channel_id=1, replica_groups=mesh['ep'=16,'tp'=16] {'ep'}, dimensions={1} | all-to-all | bytes 524288 | tf_op jit(solution)/shard_map/all_to_all | solution.py:163
  179.4 1.3 copy.86
  180.7 6.5 %all-to-all-start.6 = ((bf16[16,32,1024]{2,1,0:T(8,128)(2,1)}), bf16[16,32,1024]{2,1,0:T(8,128)(2,1)}, u32[]{:S(2)}, u32[]{:S(2)}) async-start(bf16[16,32,1024]{2,1,0:T(8,128)(2,1)} %bitcast.38), calls=%async_computation.6 | async-start | bytes 2097152 | tf_op jit(solution)/shard_map/all_to_all | solution.py:48
  187.9 0.5 broadcast_in_dim.12
  188.4 1.0 reshape.229
  189.5 13.4 %scatter_fusion = bf16[16,6,4096]{2,0,1:T(8,128)(2,1)S(1)} fusion(bf16[16,6,4096]{2,0,1:T(8,128)(2,1)S(1)} %broadcast_in_dim.11, s32[64]{0:T(128)S(1)} %get-tuple-element.28, bf16[64,4096]{1,0:T(8,128)(2,1)} %reshape.229), kind=kCustom, calls=%fused_computation.1 | custom fusion | bytes 1573376 | tf_op jit(solution)/shard_map/scatter | solution.py:192
  202.8 1.4 copy.79
  204.3 6.7 %all-to-all-start.2 = ((bf16[16,6,4096]{2,1,0:T(8,128)(2,1)}), bf16[16,6,4096]{2,1,0:T(8,128)(2,1)S(1)}, u32[]{:S(2)}, u32[]{:S(2)}) async-start(bf16[16,6,4096]{2,1,0:T(8,128)(2,1)} %copy.79), calls=%async_computation.2 | async-start | bytes 2097152 | tf_op jit(solution)/shard_map/all_to_all | solution.py:194
  211.0 1.4 convert_reduce_fusion
  212.4 12.5 %all-to-all-done.2 = bf16[16,6,4096]{2,1,0:T(8,128)(2,1)S(1)} async-done(((bf16[16,6,4096]{2,1,0:T(8,128)(2,1)}), bf16[16,6,4096]{2,1,0:T(8,128)(2,1)S(1)}, u32[]{:S(2)}, u32[]{:S(2)}) %all-to-all-start.2) | async-done | bytes 786464 | tf_op jit(solution)/shard_map/all_to_all | solution.py:194
  225.0 0.9 broadcast_in_dim.13
  225.8 6.1 %all-to-all-start.7 = ((bf16[16,32,512]{2,1,0:T(8,128)(2,1)}), bf16[16,32,512]{2,1,0:T(8,128)(2,1)}, u32[]{:S(2)}, u32[]{:S(2)}) async-start(bf16[16,32,512]{2,1,0:T(8,128)(2,1)} %broadcast_in_dim.13), calls=%async_computation.7 | async-start | bytes 1048576 | tf_op jit(solution)/shard_map/all_to_all | solution.py:20
  231.9 2.3 fusion.7
  234.2 3.8 %convolution_convert_fusion = bf16[16,6,4096]{2,0,1:T(8,128)(2,1)} fusion(bf16[1,256,4096]{2,1,0:T(8,128)(2,1)S(1)} %copy-done, bf16[1,4096,256]{2,1,0:T(8,128)(2,1)} %param.41, bf16[16,6,4096]{2,1,0:T(8,128)(2,1)S(1)} %all-to-all-done.2, f32[16,1,6,256]{3,0,2,1:T(8,128)S(1)} %fusion.7), kind=kOutput, calls=%fused_computation.2 | convolution fusion | flops 403193856 | bytes 5865472 | tf_op jit(solution)/shard_map/secf,efd->secd/dot_general | solution.py:200
  238.0 2.1 copy.102
  240.1 7.1 %all-to-all-start.3 = ((bf16[16,16,1,6,256]{4,1,3,2,0:T(8,128)(2,1)}), bf16[16,16,1,6,256]{4,1,3,2,0:T(8,128)(2,1)S(1)}, u32[]{:S(2)}, u32[]{:S(2)}) async-start(bf16[16,16,1,6,256]{4,1,3,2,0:T(8,128)(2,1)} %bitcast.130), calls=%async_computation.3 | async-start | bytes 1572864 | tf_op jit(solution)/shard_map/all_to_all | solution.py:48
  247.2 2.1 fusion.49
  249.4 20.6 %all-to-all-done.3 = bf16[16,16,1,6,256]{4,1,3,2,0:T(8,128)(2,1)S(1)} async-done(((bf16[16,16,1,6,256]{4,1,3,2,0:T(8,128)(2,1)}), bf16[16,16,1,6,256]{4,1,3,2,0:T(8,128)(2,1)S(1)}, u32[]{:S(2)}, u32[]{:S(2)}) %all-to-all-start.3) | async-done | bytes 786464 | tf_op jit(solution)/shard_map/all_to_all | solution.py:48
  269.9 6.7 %all-to-all-start.8 = ((f32[16,32,256]{2,1,0:T(8,128)}), f32[16,32,256]{2,1,0:T(8,128)}, u32[]{:S(2)}, u32[]{:S(2)}) async-start(f32[16,32,256]{2,1,0:T(8,128)} %fusion.49), calls=%async_computation.8 | async-start | bytes 1048576 | tf_op jit(solution)/shard_map/all_to_all | solution.py:181
  277.0 0.6 copy.83
  277.6 7.3 %all-to-all-done.8 = f32[16,32,256]{2,1,0:T(8,128)} async-done(((f32[16,32,256]{2,1,0:T(8,128)}), f32[16,32,256]{2,1,0:T(8,128)}, u32[]{:S(2)}, u32[]{:S(2)}) %all-to-all-start.8) | async-done | bytes 524320 | tf_op jit(solution)/shard_map/all_to_all | solution.py:181
  284.9 5.7 %all-to-all-start.4 = ((bf16[16,6,256]{2,1,0:T(8,128)(2,1)}), bf16[16,6,256]{2,1,0:T(8,128)(2,1)S(1)}, u32[]{:S(2)}, u32[]{:S(2)}) async-start(bf16[16,6,256]{2,1,0:T(8,128)(2,1)} %copy.83), calls=%async_computation.4 | async-start | bytes 131072 | tf_op jit(solution)/shard_map/all_to_all | solution.py:205
  290.7 1.9 multiply_convert_fusion
  292.5 3.0 all-to-all-done.4
  295.5 5.6 %all-to-all-start.9 = ((bf16[16,32,256]{2,1,0:T(8,128)(2,1)}), bf16[16,32,256]{2,1,0:T(8,128)(2,1)S(1)}, u32[]{:S(2)}, u32[]{:S(2)}) async-start(bf16[16,32,256]{2,1,0:T(8,128)(2,1)} %multiply_convert_fusion), calls=%async_computation.9 | async-start | bytes 524288 | tf_op jit(solution)/shard_map/all_to_all | solution.py:48
  301.2 0.9 gather_fusion
  302.3 10.4 %all-to-all-done.9 = bf16[16,32,256]{2,1,0:T(8,128)(2,1)S(1)} async-done(((bf16[16,32,256]{2,1,0:T(8,128)(2,1)}), bf16[16,32,256]{2,1,0:T(8,128)(2,1)S(1)}, u32[]{:S(2)}, u32[]{:S(2)}) %all-to-all-start.9) | async-done | bytes 262176 | tf_op jit(solution)/shard_map/all_to_all | solution.py:48
  312.7 0.7 add_convert_fusion
  313.4 14.4 %all_to_all.85 = bf16[16,32,256]{2,1,0:T(8,128)(2,1)S(1)} all-to-all(bf16[16,32,256]{2,1,0:T(8,128)(2,1)S(1)} %broadcast_in_dim.14), channel_id=1, replica_groups=mesh['ep'=16,'tp'=16] {'tp'}, dimensions={0} | all-to-all | bytes 524288 | tf_op jit(solution)/shard_map/all_to_all | solution.py:20
  327.8 0.7 copy.93
  (73 shorter events, 3.3 us)
Async XLA Ops:
  7.2 227.0 %copy-start = (bf16[1,256,4096]{2,1,0:T(8,128)(2,1)S(1)}, bf16[1,256,4096]{2,1,0:T(8,128)(2,1)}, u32[]{:S(2)}) copy-start(bf16[1,256,4096]{2,1,0:T(8,128)(2,1)} %param.42) | copy-start | bytes 6291460
  7.2 62.9 %copy-start.4 = (bf16[32,4096]{1,0:T(8,128)(2,1)S(1)}, bf16[32,4096]{1,0:T(8,128)(2,1)}, u32[]{:S(2)}) copy-start(bf16[32,4096]{1,0:T(8,128)(2,1)} %param.23) | copy-start | bytes 786436
  7.2 62.9 %copy-start.16 = (f32[4096]{0:T(1024)S(1)}, f32[4096]{0:T(1024)}, u32[]{:S(2)}) copy-start(f32[4096]{0:T(1024)} %param.27) | copy-start | bytes 49156
  7.2 6.8 %copy-start.14 = (f32[32,1]{0,1:T(1,128)S(1)}, f32[32,1]{0,1:T(1,128)}, u32[]{:S(2)}) copy-start(f32[32,1]{0,1:T(1,128)} %param.26) | copy-start | bytes 388
  7.2 64.6 %copy-start.15 = (f32[32,1,128]{2,1,0:T(1,128)S(1)}, f32[32,1,128]{2,1,0:T(1,128)}, u32[]{:S(2)}) copy-start(f32[32,1,128]{2,1,0:T(1,128)} %param.25) | copy-start | bytes 49156
  7.2 62.8 %all-gather.3.cloned.1.call-start = ((), (), s32[]{:S(2)}) async-start(), calls=%async_computation.11 | async-start | bytes 4456448 | tf_op jit(solution)/shard_map/all_gather | solution.py:15
  9.1 152.8 %all-gather.5.cloned.1.call-start = ((), (), s32[]{:S(2)}) async-start(), calls=%async_computation.12 | async-start | bytes 8912896 | tf_op jit(solution)/shard_map/all_gather | solution.py:37
  14.7 60.8 %copy-start.12 = (f32[32,1]{0,1:T(1,128)}, f32[32,1]{0,1:T(1,128)S(1)}, u32[]{:S(2)}) copy-start(f32[32,1]{0,1:T(1,128)S(1)} %get-tuple-element.35) | copy-start | bytes 388
  70.1 5.5 %copy-start.2 = (f32[32,1,128,128]{3,2,1,0:T(8,128)S(1)}, f32[32,1,128,128]{3,2,1,0:T(8,128)}, u32[]{:S(2)}) copy-start(f32[32,1,128,128]{3,2,1,0:T(8,128)} %param.24) | copy-start | bytes 6291460
  76.4 13.2 %copy-start.1 = (f32[32,1,128,128]{3,2,1,0:T(8,128)}, f32[32,1,128,128]{3,2,1,0:T(8,128)S(1)}, u32[]{:S(2)}) copy-start(f32[32,1,128,128]{3,2,1,0:T(8,128)S(1)} %multiply_add_fusion) | copy-start | bytes 6291460
  76.4 13.2 %copy-start.8 = (bf16[128,256]{1,0:T(8,128)(2,1)S(1)}, bf16[128,256]{1,0:T(8,128)(2,1)}, u32[]{:S(2)}) copy-start(bf16[128,256]{1,0:T(8,128)(2,1)} %param.35) | copy-start | bytes 196612
  103.4 62.6 %copy-start.9 = (f32[4096]{0:T(1024)S(1)}, f32[4096]{0:T(1024)}, u32[]{:S(2)}) copy-start(f32[4096]{0:T(1024)} %param.36) | copy-start | bytes 49156
  165.8 12.8 %copy-start.6 = (bf16[256,512]{1,0:T(8,128)(2,1)S(1)}, bf16[256,512]{1,0:T(8,128)(2,1)}, u32[]{:S(2)}) copy-start(bf16[256,512]{1,0:T(8,128)(2,1)} %param.44) | copy-start | bytes 786436
  165.8 13.1 %copy-start.7 = (bf16[256,512]{1,0:T(8,128)(2,1)S(1)}, bf16[256,512]{1,0:T(8,128)(2,1)}, u32[]{:S(2)}) copy-start(bf16[256,512]{1,0:T(8,128)(2,1)} %param.43) | copy-start | bytes 786436
  166.0 12.9 %copy-start.3 = (bf16[32,4096]{1,0:T(8,128)(2,1)}, bf16[32,4096]{1,0:T(8,128)(2,1)S(1)}, u32[]{:S(2)}) copy-start(bf16[32,4096]{1,0:T(8,128)(2,1)S(1)} %get-tuple-element.31) | copy-start | bytes 786436
  179.4 7.9 %copy-start.13 = (s32[32,2]{0,1:T(2,128)S(1)}, s32[32,2]{0,1:T(2,128)}, u32[]{:S(2)}) copy-start(s32[32,2]{0,1:T(2,128)} %param.38) | copy-start | bytes 772
  180.7 23.6 %all-to-all-start.6 = ((bf16[16,32,1024]{2,1,0:T(8,128)(2,1)}), bf16[16,32,1024]{2,1,0:T(8,128)(2,1)}, u32[]{:S(2)}, u32[]{:S(2)}) async-start(bf16[16,32,1024]{2,1,0:T(8,128)(2,1)} %bitcast.38), calls=%async_computation.6 | async-start | bytes 2097152 | tf_op jit(solution)/shard_map/all_to_all | solution.py:48
  204.3 20.7 %all-to-all-start.2 = ((bf16[16,6,4096]{2,1,0:T(8,128)(2,1)}), bf16[16,6,4096]{2,1,0:T(8,128)(2,1)S(1)}, u32[]{:S(2)}, u32[]{:S(2)}) async-start(bf16[16,6,4096]{2,1,0:T(8,128)(2,1)} %copy.79), calls=%async_computation.2 | async-start | bytes 2097152 | tf_op jit(solution)/shard_map/all_to_all | solution.py:194
  225.8 14.3 %all-to-all-start.7 = ((bf16[16,32,512]{2,1,0:T(8,128)(2,1)}), bf16[16,32,512]{2,1,0:T(8,128)(2,1)}, u32[]{:S(2)}, u32[]{:S(2)}) async-start(bf16[16,32,512]{2,1,0:T(8,128)(2,1)} %broadcast_in_dim.13), calls=%async_computation.7 | async-start | bytes 1048576 | tf_op jit(solution)/shard_map/all_to_all | solution.py:20
  238.0 9.3 %copy-start.5 = (bf16[512,256]{1,0:T(8,128)(2,1)S(1)}, bf16[512,256]{1,0:T(8,128)(2,1)}, u32[]{:S(2)}) copy-start(bf16[512,256]{1,0:T(8,128)(2,1)} %param.45) | copy-start | bytes 786436
  240.1 36.5 %copy-start.11 = (f32[32,2]{0,1:T(2,128)S(1)}, f32[32,2]{0,1:T(2,128)}, u32[]{:S(2)}) copy-start(f32[32,2]{0,1:T(2,128)} %param.39) | copy-start | bytes 772
  240.1 36.5 %copy-start.10 = (bf16[4096]{0:T(1024)(128)(2,1)S(1)}, bf16[4096]{0:T(1024)(128)(2,1)}, u32[]{:S(2)}) copy-start(bf16[4096]{0:T(1024)(128)(2,1)} %param.37) | copy-start | bytes 24580
  240.1 29.8 %all-to-all-start.3 = ((bf16[16,16,1,6,256]{4,1,3,2,0:T(8,128)(2,1)}), bf16[16,16,1,6,256]{4,1,3,2,0:T(8,128)(2,1)S(1)}, u32[]{:S(2)}, u32[]{:S(2)}) async-start(bf16[16,16,1,6,256]{4,1,3,2,0:T(8,128)(2,1)} %bitcast.130), calls=%async_computation.3 | async-start | bytes 1572864 | tf_op jit(solution)/shard_map/all_to_all | solution.py:48
  269.9 15.0 %all-to-all-start.8 = ((f32[16,32,256]{2,1,0:T(8,128)}), f32[16,32,256]{2,1,0:T(8,128)}, u32[]{:S(2)}, u32[]{:S(2)}) async-start(f32[16,32,256]{2,1,0:T(8,128)} %fusion.49), calls=%async_computation.8 | async-start | bytes 1048576 | tf_op jit(solution)/shard_map/all_to_all | solution.py:181
  284.9 10.5 %all-to-all-start.4 = ((bf16[16,6,256]{2,1,0:T(8,128)(2,1)}), bf16[16,6,256]{2,1,0:T(8,128)(2,1)S(1)}, u32[]{:S(2)}, u32[]{:S(2)}) async-start(bf16[16,6,256]{2,1,0:T(8,128)(2,1)} %copy.83), calls=%async_computation.4 | async-start | bytes 131072 | tf_op jit(solution)/shard_map/all_to_all | solution.py:205
  295.5 17.2 %all-to-all-start.9 = ((bf16[16,32,256]{2,1,0:T(8,128)(2,1)}), bf16[16,32,256]{2,1,0:T(8,128)(2,1)S(1)}, u32[]{:S(2)}, u32[]{:S(2)}) async-start(bf16[16,32,256]{2,1,0:T(8,128)(2,1)} %multiply_convert_fusion), calls=%async_computation.9 | async-start | bytes 524288 | tf_op jit(solution)/shard_map/all_to_all | solution.py:48
Sparse Core Ops, SparseCore 0:
  11.0 58.9 all-gather.2
  103.6 58.3 all-gather.4
where the time goes:
time: 340 us; the launch traced here: 335 us
  waiting for transfers between devices  168 us (49%)
  blocking collectives  48.9 us (14%)
  starting transfers between devices  44.4 us (13%)
  local copies, waits for them, and re-layouts  26 us (8%)
  matrix products  20.7 us (6%)
  between operations  14.4 us (4%)
  other arithmetic  13.4 us (4%)
    all_gather x1, waiting for transfers between devices, total_of_pieces(): return lax.all_gather(shard, axis).sum(0)  58.5 us
    all_gather x1, waiting for transfers between devices, side_by_side(): lax.all_gather(both, axis, axis=dim, tiled=True)  55.3 us
    all_to_all x3, waiting for transfers between devices, sum_at_owner(): lax.all_to_all(parts, axis, split_axis=0, concat_axis=0, tiled=True)  31 us
    all_to_all x2, blocking collectives, from_everyone(): lax.all_to_all(jnp.broadcast_to(shard[None], (devices, *shard.shape)), ax...  24 us
    all_to_all x3, starting transfers between devices, sum_at_owner(): lax.all_to_all(parts, axis, split_axis=0, concat_axis=0, tiled=True)  19.2 us
    scatter x2, local copies, waits for them, and re-layouts, on_device(): outbound = jnp.zeros((experts_all, capacity, model_width), jnp.bfloat16)....  14.8 us
    all_to_all x1, waiting for transfers between devices, on_device(): lax.all_to_all(outbound, 'ep', split_axis=0, concat_axis=0, tiled=True)  12.5 us
    all_to_all x1, blocking collectives, on_device(): lax.all_to_all(spread_out, 'ep', split_axis=0, concat_axis=1, tiled=True)  12.4 us
  transfers between devices with their start and end apart: 9, of which 7 were waited for; matrix products, arithmetic and copies ran while one was open for 11% of the time, Pallas kernels for 0%

commit v1 on v0

v1 whole, which is shorter than its diff:
```python
import functools

import jax
import jax.numpy as jnp
from jax import lax
from jax.experimental import pallas as pl
from jax.experimental.pallas import tpu as pltpu
from jax.sharding import PartitionSpec as P

EPS = 1e-06
MESH = pl.DeviceIdType.MESH
F32 = jnp.float32
BF16 = jnp.bfloat16
N = 16
NZ = 8
ROWS = 32
D = 4096
COLS = 256
HALF = 2048
HD = 128


def dot(a, b):
    return jnp.dot(a, b, preferred_element_type=F32)


def dot_rows(a, b):
    return lax.dot_general(a, b, (((1,), (1,)), ((), ())), preferred_element_type=F32)


def layer_kernel(
    tok_h, st_h, sn_h, smax_h, gmix_h, wq_h, wk_h, wv_h, wo_h, wi_h, wf_h, fb_h, wp_h, gffn_h, wbr_h,
    rt_h, rw_h, eg_h, eu_h, ed_h, dg_h, du_h, dd_h,
    out_h, nm_h, nn_h, nmax_h,
    tok, st, sn, smax, gmix, wq, wi, wf, fb, wp, gffn, wbr, rt, rw, eg, eu, ed, dgu, dd,
    xall, csend, crecv, mhall, num,
    part, pd2d, rsend, rrecv, resall,
    part2, pd2d2, rsend2, rrecv2,
    rtsend, rtall, dsend, drecv, stsend, strecv, hall, r2all, aall,
    xs, xfull, aexp, acc, yp, yd2d, ys, yrecv, yout, ycomb, outv, nnv, nmaxv,
    load_sem, ssem, bsem, rsem, zsem, z2sem, store_sem,
):
    e = lax.axis_index("ep")
    t = lax.axis_index("tp")
    z = t // 2
    c = lax.rem(t, 2)
    mate = 2 * z + 1 - c

    def rcopy(src, dst, send, recv, pe, pt):
        return pltpu.make_async_remote_copy(
            src_ref=src, dst_ref=dst, send_sem=send, recv_sem=recv, device_id=(pe, pt), device_id_type=MESH
        )

    def wait_for(ref, sem):
        pltpu.make_async_copy(ref, ref, sem).wait()

    def either(less, ref_less, ref_all, sem):
        @pl.when(less)
        def _():
            wait_for(ref_less, sem)

        @pl.when(jnp.logical_not(less))
        def _():
            wait_for(ref_all, sem)

    def up(d):
        return lax.rem(e + d, N)

    def down(d):
        return lax.rem(e + N - d, N)

    def over_ep(fn):
        lax.fori_loop(1, N, lambda d, carry: (fn(up(d)), carry)[1], 0)

    def over_z(fn):
        lax.fori_loop(1, NZ, lambda d, carry: (fn(lax.rem(z + d, NZ)), carry)[1], 0)

    def cols(index):
        return pl.ds(pl.multiple_of(index * COLS, COLS), COLS)

    def half(index):
        return pl.ds(pl.multiple_of(index * HALF, HALF), HALF)

    loads = [
        (tok_h, tok), (gmix_h, gmix),
        (wq_h, wq.at[:, 0:128]), (wk_h, wq.at[:, 128:256]), (wv_h, wq.at[:, 256:384]), (wo_h, wq.at[:, 384:512]),
        (wi_h, wi), (wf_h, wf), (fb_h, fb), (smax_h, smax), (sn_h, sn), (st_h, st), (wp_h, wp), (gffn_h, gffn),
        (wbr_h, wbr), (rt_h, rt), (rw_h, rw), (dg_h, dgu.at[:, 0:512]), (du_h, dgu.at[:, 512:1024]), (dd_h, dd),
        (eg_h.at[0], eg), (eu_h.at[0], eu), (ed_h.at[0], ed),
    ]
    copies = [pltpu.make_async_copy(s, d, load_sem.at[i]) for i, (s, d) in enumerate(loads)]
    for copy in copies:
        copy.start()

    barrier = pltpu.get_barrier_semaphore()

    def greet_ep(p):
        pl.semaphore_signal(barrier, inc=1, device_id=(p, t), device_id_type=MESH)

    def greet_tp(d, carry):
        pl.semaphore_signal(barrier, inc=1, device_id=(e, lax.rem(t + d, N)), device_id_type=MESH)
        return carry

    over_ep(greet_ep)
    lax.fori_loop(1, N, greet_tp, 0)
    copies[0].wait()
    copies[1].wait()
    pl.semaphore_wait(barrier, 2 * (N - 1))

    over_ep(lambda p: rcopy(tok.at[:, cols(p)], xall.at[e], ssem.at[0], bsem.at[e], p, t).start())
    xall[e] = tok[:, cols(e)]
    gain_e = gmix[:, cols(e)]

    total = jnp.zeros((ROWS, 128), F32)
    for k in range(8):
        wide = tok[:, k * 512:(k + 1) * 512].astype(F32)
        sq = wide * wide
        total = total + (sq[:, 0:128] + sq[:, 128:256]) + (sq[:, 256:384] + sq[:, 384:512])
    rstd = lax.rsqrt(jnp.sum(total, axis=1, keepdims=True) * (1.0 / D) + EPS)
    for i in (6, 7, 8, 9, 15, 16):
        copies[i].wait()
    gi = jnp.zeros((ROWS, N), F32)
    gf = jnp.zeros((ROWS, N), F32)
    for k in range(8):
        cut = slice(k * 512, (k + 1) * 512)
        nb = (tok[:, cut].astype(F32) * rstd * gmix[:, cut]).astype(BF16)
        gi = gi + dot(nb, wi[cut, :])
        gf = gf + dot(nb, wf[cut, :])
    gf = gf + fb[...]
    mine = lax.broadcasted_iota(jnp.int32, (ROWS, N), 1) == t
    gate_in = jnp.sum(jnp.where(mine, gi, 0.0), axis=1, keepdims=True)
    gate_f = jnp.sum(jnp.where(mine, gf, 0.0), axis=1, keepdims=True)
    log_keep = jnp.minimum(gate_f, 0.0) - jnp.log1p(jnp.exp(-jnp.abs(gate_f)))
    kept = log_keep + smax[...]
    new_max = jnp.maximum(kept, gate_in)
    keep = jnp.exp(kept - new_max)
    write = jnp.exp(gate_in - new_max)
    nmaxv[...] = new_max
    lane = lax.broadcasted_iota(jnp.int32, (ROWS, 128), 1)
    r_in = rt[...].astype(F32)
    w_in = rw[...]
    packed = jnp.where(lane == 0, r_in[:, 0:1], jnp.where(lane == 1, r_in[:, 1:2], jnp.where(lane == 2, w_in[:, 0:1], w_in[:, 1:2])))
    wide_rt = jnp.concatenate([packed, jnp.full((96, 128), -1.0, F32)], axis=0)
    rtsend[...] = jnp.transpose(wide_rt)[0:8, :]
    over_ep(lambda p: rcopy(rtsend, rtall.at[e], ssem.at[1], rsem.at[0], p, t).start())
    rtall[e] = rtsend[...]
    for i in (2, 3, 4, 5, 10, 11):
        copies[i].wait()

    for g in range(4):
        ps = [down(4 * g + j) for j in range(4)]
        for j in range(4):
            if 4 * g + j:
                wait_for(xall.at[ps[j]], bsem.at[ps[j]])
        block = jnp.concatenate([xall[p] for p in ps], axis=0)
        prod = dot((block.astype(F32) * gain_e).astype(BF16), wq[...])
        for j in range(4):
            piece = prod[32 * j:32 * j + 32].astype(BF16)
            if 4 * g + j:
                csend[ps[j]] = piece
                rcopy(csend.at[ps[j]], crecv.at[e], ssem.at[2], rsem.at[1], ps[j], t).start()
            else:
                crecv[e] = piece
    wait_for(crecv.at[0:15], rsem.at[1])
    qkvo = crecv[0].astype(F32)
    for i in range(1, N):
        qkvo = qkvo + crecv[i].astype(F32)
    qkvo = qkvo * rstd
    q = qkvo[:, 0:128]
    kw = qkvo[:, 128:256] * (HD ** -0.5) * write
    v = qkvo[:, 256:384]
    keep_w = jnp.broadcast_to(keep, (ROWS, HD))
    new_norm = keep_w * sn[...] + kw
    nnv[...] = new_norm
    kw_t = jnp.transpose(kw)
    q_t = jnp.transpose(q)
    for b in range(ROWS):
        new = keep_w[b:b + 1, :] * st[b] + kw_t[:, b:b + 1] * v[b:b + 1, :]
        st[b] = new
        num[b:b + 1, :] = jnp.sum(q_t[:, b:b + 1] * new, axis=0, keepdims=True)
    denom = jnp.maximum(jnp.abs(jnp.sum(q * new_norm, axis=1, keepdims=True)), 1.0)
    mixed = (jax.nn.sigmoid(qkvo[:, 384:512]) * (num[...] / denom)).astype(BF16)
    mhall[e] = mixed
    over_ep(lambda p: rcopy(mhall.at[e], mhall.at[e], ssem.at[3], rsem.at[2], p, t).start())
    stores = [
        pltpu.make_async_copy(st, nm_h, store_sem.at[0]),
        pltpu.make_async_copy(nnv, nn_h, store_sem.at[1]),
        pltpu.make_async_copy(nmaxv, nmax_h, store_sem.at[2]),
    ]
    for store in stores:
        store.start()

    wait_for(rtall.at[0:15], rsem.at[0])
    before = (lax.broadcasted_iota(jnp.int32, (128, 128), 0) < lax.broadcasted_iota(jnp.int32, (128, 128), 1)).astype(BF16)
    row8 = lax.broadcasted_iota(jnp.int32, (128, 128), 0)
    row_e = (row8 // 8).astype(F32)
    row_s = lax.rem(row8, 8).astype(F32)

    def table(group):
        info = rtall[group]
        first = (info[0:1, :] == row_e).astype(F32)
        second = (info[1:2, :] == row_e).astype(F32)
        slot = dot((first + second).astype(BF16), before)
        fits = (slot == row_s).astype(F32)
        share = 1.0 / (info[2:3, :] + info[3:4, :])
        pick = (first + second) * fits
        weigh = (first * (info[2:3, :] * share) + second * (info[3:4, :] * share)) * fits
        return pick[:, 0:ROWS], weigh

    pick0, weigh0 = table(2 * z)
    pick1, weigh1 = table(2 * z + 1)
    weigh = jnp.where(c == 0, weigh0, weigh1)
    weigh_t = jnp.transpose(weigh)[0:ROWS, :]

    copies[12].wait()
    wait_for(mhall.at[0:15], rsem.at[2])

    def reduce_tp(parts, recv, send, zrecv, s, r):
        copy = rcopy(parts.at[:, 1 - c], recv, ssem.at[s], rsem.at[r], e, mate)
        copy.start()
        wait_for(recv, rsem.at[r])
        for k in range(NZ):
            send[k] = (parts[k, c].astype(F32) + recv[k].astype(F32)).astype(BF16)
        over_z(lambda p: rcopy(send.at[p], zrecv.at[z], ssem.at[s + 1], rsem.at[r + 1], e, 2 * p + c).start())
        zrecv[z] = send[z]

    def total_tp(zrecv, r):
        wait_for(zrecv.at[0:7], rsem.at[r + 1])
        tot = zrecv[0].astype(F32)
        for k in range(1, NZ):
            tot = tot + zrecv[k].astype(F32)
        return tot

    for g in range(4):
        block = jnp.concatenate([mhall[4 * g + j] for j in range(4)], axis=0)
        prod = dot(block, wp[...])
        for j in range(4):
            b = 4 * g + j
            part[b // 2, b % 2] = prod[32 * j:32 * j + 32].astype(BF16)
    reduce_tp(part, pd2d, rsend, rrecv, 4, 3)
    mix = total_tp(rrecv, 3)
    res_own = (xall[t].astype(F32) + mix).astype(BF16)
    resall[z, c] = res_own

    rcopy(resall.at[z, c], resall.at[z, c], ssem.at[6], z2sem.at[0, z], e, mate).start()
    over_z(lambda p: rcopy(resall.at[z, c], resall.at[z, c], ssem.at[7], zsem.at[0, z], e, 2 * p + c).start())
    wait_for(resall.at[z, 1 - c], z2sem.at[0, z])
    both = jnp.concatenate([resall[z, 0], resall[z, 1]], axis=0)
    zero = jnp.zeros((8, ROWS), F32)
    spread = []
    for ex in range(N):
        spread.append(jnp.concatenate([pick0[8 * ex:8 * ex + 8], zero], axis=1))
        spread.append(jnp.concatenate([zero, pick1[8 * ex:8 * ex + 8]], axis=1))
    routed = dot(jnp.concatenate(spread, axis=0).astype(BF16), both).astype(BF16)
    for ex in range(N):
        xs[ex] = routed[16 * ex:16 * ex + 16]
    over_ep(lambda p: rcopy(xs.at[p], xfull.at[z, :, cols(e)], ssem.at[8], rsem.at[5], p, t).start())
    xfull[z, :, cols(e)] = xs[e]

    for i in (13, 14, 17, 18):
        copies[i].wait()
    for d in range(1, NZ):
        p = lax.rem(z + NZ - d, NZ)
        wait_for(resall.at[p, c], zsem.at[0, p])
        rcopy(resall.at[p, c], resall.at[p, c], ssem.at[9], z2sem.at[0, p], e, mate).start()

    wait_for(xs.at[0:15], rsem.at[5])
    over_z(lambda p: rcopy(xfull.at[z, :, half(c)], xfull.at[z, :, half(c)], ssem.at[10], zsem.at[1, z], e, 2 * p + c).start())

    gain_f = gffn[:, cols(e)]
    w_b = wbr[:, cols(e)].astype(BF16)
    for d in range(1, NZ):
        p = lax.rem(z + NZ - d, NZ)
        wait_for(resall.at[p, 1 - c], z2sem.at[0, p])
    for k in range(NZ):
        wide = jnp.concatenate([resall[k, 0], resall[k, 1]], axis=0).astype(F32)
        r2all[64 * k:64 * k + 64] = (wide * wide).astype(BF16)
        aall[64 * k:64 * k + 64] = (wide * gain_f).astype(BF16)

    def dense_block(g, carry):
        rows = pl.ds(pl.multiple_of(g * 128, 128), 128)
        lhs = aall[rows, :]
        for h in range(2):
            prod = dot(lhs, dgu[:, 512 * h:512 * h + 512])
            for j in range(4):
                dsend[4 * g + j, :, 512 * h:512 * h + 512] = prod[32 * j:32 * j + 32].astype(BF16)
        stat = dot_rows(jnp.ones((8, COLS), BF16), r2all[rows, :])
        br = dot_rows(jnp.broadcast_to(w_b, (8, COLS)), lhs)
        sub = lax.broadcasted_iota(jnp.int32, (8, 128), 0)
        stsend[g] = jnp.where(sub < 4, stat, br)
        return carry

    lax.fori_loop(0, 4, dense_block, 0)
    over_ep(lambda p: rcopy(dsend.at[p], drecv.at[e], ssem.at[11], rsem.at[6], p, t).start())
    over_ep(lambda p: rcopy(stsend.at[p // 4], strecv.at[e], ssem.at[12], rsem.at[7], p, t).start())
    drecv[e] = dsend[e]
    strecv[e] = stsend[e // 4]

    for d in range(1, NZ):
        p = lax.rem(z + NZ - d, NZ)
        wait_for(xfull.at[p, :, half(c)], zsem.at[1, p])
        rcopy(xfull.at[p, :, half(c)], xfull.at[p, :, half(c)], ssem.at[13], z2sem.at[1, p], e, mate).start()

    wait_for(drecv.at[0:15], rsem.at[6])
    wait_for(strecv.at[0:15], rsem.at[7])
    stats = strecv[0]
    for i in range(1, N):
        stats = stats + strecv[i]
    at = lane == lax.broadcasted_iota(jnp.int32, (ROWS, 128), 0) + ROWS * lax.rem(e, 4)
    sumsq = jnp.sum(jnp.where(at, stats[0:1, :], 0.0), axis=1, keepdims=True)
    branch = jnp.sum(jnp.where(at, stats[4:5, :], 0.0), axis=1, keepdims=True)
    rstd2 = lax.rsqrt(sumsq * (1.0 / D) + EPS)
    branch_share = jax.nn.sigmoid(branch * rstd2)
    for h in range(2):
        cg = slice(256 * h, 256 * h + 256)
        cu = slice(512 + 256 * h, 512 + 256 * h + 256)
        g_ = drecv[0, :, cg].astype(F32)
        u_ = drecv[0, :, cu].astype(F32)
        for i in range(1, N):
            g_ = g_ + drecv[i, :, cg].astype(F32)
            u_ = u_ + drecv[i, :, cu].astype(F32)
        g_ = g_ * rstd2
        u_ = u_ * rstd2
        hall[e, :, cg] = (g_ * jax.nn.sigmoid(g_) * u_ * branch_share).astype(BF16)
    over_ep(lambda p: rcopy(hall.at[e], hall.at[e], ssem.at[14], rsem.at[8], p, t).start())

    for i in (20, 21, 22):
        copies[i].wait()
    for d in range(1, NZ):
        p = lax.rem(z + NZ - d, NZ)
        wait_for(xfull.at[p, :, half(1 - c)], z2sem.at[1, p])

    def expert_rows(k, carry):
        tot = jnp.zeros((16, 128), F32)
        for m in range(4):
            wide = xfull[k, :, 1024 * m:1024 * m + 1024].astype(F32)
            sq = wide * wide
            for n in range(8):
                tot = tot + sq[:, 128 * n:128 * n + 128]
        scale = lax.rsqrt(jnp.sum(tot, axis=1, keepdims=True) * (1.0 / D) + EPS)
        rows = pl.ds(pl.multiple_of(k * 16, 16), 16)
        for m in range(4):
            cut = slice(1024 * m, 1024 * m + 1024)
            aexp[rows, cut] = (xfull[k, :, cut].astype(F32) * scale * gffn[:, cut]).astype(BF16)
        return carry

    lax.fori_loop(0, NZ, expert_rows, 0)
    acc[...] = jnp.zeros_like(acc)

    def expert_in(k, carry):
        cut = pl.ds(pl.multiple_of(k * 512, 512), 512)
        lhs = aexp[:, cut]
        acc[:, 0:256] += dot(lhs, eg[cut, :])
        acc[:, 256:512] += dot(lhs, eu[cut, :])
        return carry

    lax.fori_loop(0, 8, expert_in, 0)
    g_ = acc[:, 0:256]
    hid = (g_ * jax.nn.sigmoid(g_) * acc[:, 256:512]).astype(BF16)
    aexp[:, 0:256] = hid

    def expert_out(k, carry):
        cut = pl.ds(pl.multiple_of(k * 512, 512), 512)
        prod = dot(aexp[:, 0:256], ed[:, cut]).astype(BF16)
        for n in range(NZ):
            yp[n, :, cut] = prod[16 * n:16 * n + 16]
        return carry

    lax.fori_loop(0, 8, expert_out, 0)
    rcopy(yp.at[:, :, half(1 - c)], yd2d, ssem.at[15], rsem.at[9], e, mate).start()

    copies[19].wait()
    wait_for(hall.at[0:15], rsem.at[8])

    def dense_down(g, carry):
        block = jnp.concatenate([hall[4 * g + j] for j in range(4)], axis=0)
        prod = dot(block, dd[...])
        for j in range(4):
            part2[2 * g + j // 2, j % 2] = prod[32 * j:32 * j + 32].astype(BF16)
        return carry

    lax.fori_loop(0, 4, dense_down, 0)
    reduce_tp(part2, pd2d2, rsend2, rrecv2, 16, 10)

    wait_for(yd2d, rsem.at[9])

    def sum_pair(k, carry):
        ys[k] = (yp[k, :, half(c)].astype(F32) + yd2d[k].astype(F32)).astype(BF16)
        return carry

    lax.fori_loop(0, NZ, sum_pair, 0)
    over_z(lambda p: rcopy(ys.at[p], yrecv.at[z], ssem.at[18], rsem.at[12], e, 2 * p + c).start())
    yrecv[z] = ys[z]
    dense = total_tp(rrecv2, 10)
    wait_for(yrecv.at[0:7], rsem.at[12])
    for m in range(4):
        cut = slice(512 * m, 512 * m + 512)
        tot = yrecv[0, :, cut].astype(F32)
        for k in range(1, NZ):
            tot = tot + yrecv[k, :, cut].astype(F32)
        yout[:, cut] = tot.astype(BF16)

    def back(j, carry):
        src = yout.at[:, pl.ds(pl.multiple_of(j * COLS, COLS), COLS)]
        pe = c * NZ + j
        rcopy(src, ycomb.at[e], ssem.at[19], rsem.at[13], pe, mate).start()

        @pl.when(pe != e)
        def _():
            rcopy(src, ycomb.at[e], ssem.at[20], rsem.at[13], pe, t).start()

        @pl.when(pe == e)
        def _():
            ycomb[e] = yout[:, pl.ds(pl.multiple_of(j * COLS, COLS), COLS)]

        return carry

    lax.fori_loop(0, NZ, back, 0)
    either(e // NZ == c, ycomb.at[0:15], ycomb, rsem.at[13])

    picked = jnp.concatenate([ycomb[ex, :, :] for ex in range(N)], axis=0).astype(F32)
    own = jnp.concatenate([picked[16 * ex:16 * ex + 16].reshape(2, 8, COLS) for ex in range(N)], axis=0)
    sel = jnp.concatenate(
        [jnp.where(c == 0, own[2 * ex], own[2 * ex + 1]) for ex in range(N)], axis=0
    )
    high = weigh_t.astype(BF16)
    low = (weigh_t - high.astype(F32)).astype(BF16)
    sel16 = sel.astype(BF16)
    mixed_out = dot(high, sel16) + dot(low, sel16)
    outv[...] = (resall[z, c].astype(F32) + mixed_out + dense).astype(BF16)

    def deliver(d, carry):
        pt = lax.rem(t + d, N)

        @pl.when(jnp.logical_or(t != e, pt != t))
        def _():
            rcopy(outv, out_h.at[:, cols(e)], ssem.at[21], rsem.at[14], t, pt).start()

        return carry

    lax.fori_loop(0, N, deliver, 0)

    @pl.when(t == e)
    def _():
        own_copy = pltpu.make_async_copy(outv, out_h.at[:, cols(e)], store_sem.at[3])
        own_copy.start()
        own_copy.wait()

    either(t == e, out_h.at[:, 0:15 * COLS], out_h, rsem.at[14])

    wait_for(xall.at[0:15], ssem.at[0])
    wait_for(rtall.at[0:15], ssem.at[1])
    wait_for(csend.at[0:15], ssem.at[2])
    wait_for(mhall.at[0:15], ssem.at[3])
    wait_for(pd2d, ssem.at[4])
    wait_for(rsend.at[0:7], ssem.at[5])
    wait_for(resall.at[0, 0], ssem.at[6])
    wait_for(rsend.at[0:7], ssem.at[7])
    wait_for(xs.at[0:15], ssem.at[8])
    wait_for(rsend.at[0:7], ssem.at[9])
    wait_for(ys.at[0:7], ssem.at[10])
    wait_for(dsend.at[0:15], ssem.at[11])
    wait_for(strecv.at[0:15], ssem.at[12])
    wait_for(ys.at[0:7], ssem.at[13])
    wait_for(hall.at[0:15], ssem.at[14])
    wait_for(yd2d, ssem.at[15])
    wait_for(pd2d2, ssem.at[16])
    wait_for(rsend2.at[0:7], ssem.at[17])
    wait_for(ys.at[0:7], ssem.at[18])
    wait_for(ycomb.at[0:8], ssem.at[19])
    either(e // NZ == c, ycomb.at[0:7], ycomb.at[0:8], ssem.at[20])

    either(t == e, xall.at[0:15], xall, ssem.at[21])

    for store in stores:
        store.wait()


def on_device(
    tokens, state_matrix, state_norm, state_max, mixer_gain, w_query, w_key, w_value, w_outgate, w_ingate, w_forget,
    forget_bias, w_proj, ffn_gain, w_branch, routes, route_weight, expert_gate, expert_up, expert_down,
    dense_gate, dense_up, dense_down,
):
    any_ = pl.BlockSpec(memory_space=pl.ANY)
    vm = pltpu.VMEM
    scratch = [
        vm((ROWS, D), BF16), vm((ROWS, HD, HD), F32), vm((ROWS, HD), F32), vm((ROWS, 1), F32), vm((1, D), F32),
        vm((COLS, 512), BF16), vm((D, N), BF16), vm((D, N), BF16), vm((1, N), F32), vm((HD, COLS), BF16),
        vm((1, D), F32), vm((1, D), F32), vm((ROWS, 2), jnp.int32), vm((ROWS, 2), F32),
        vm((D, COLS), BF16), vm((D, COLS), BF16), vm((COLS, D), BF16), vm((COLS, 1024), BF16), vm((512, COLS), BF16),
        vm((N, ROWS, COLS), BF16), vm((N, ROWS, 512), BF16), vm((N, ROWS, 512), BF16), vm((N, ROWS, HD), BF16),
        vm((ROWS, HD), F32),
        vm((NZ, 2, ROWS, COLS), BF16), vm((NZ, ROWS, COLS), BF16), vm((NZ, ROWS, COLS), BF16),
        vm((NZ, ROWS, COLS), BF16), vm((NZ, 2, ROWS, COLS), BF16),
        vm((NZ, 2, ROWS, COLS), BF16), vm((NZ, ROWS, COLS), BF16), vm((NZ, ROWS, COLS), BF16),
        vm((NZ, ROWS, COLS), BF16),
        vm((8, 128), F32), vm((N, 8, 128), F32), vm((N, ROWS, 1024), BF16), vm((N, ROWS, 1024), BF16),
        vm((4, 8, 128), F32), vm((N, 8, 128), F32), vm((N, ROWS, 512), BF16), vm((512, COLS), BF16),
        vm((512, COLS), BF16),
        vm((N, 16, COLS), BF16), vm((NZ, 16, D), BF16), vm((128, D), BF16), vm((128, 512), F32),
        vm((NZ, 16, D), BF16), vm((NZ, 16, HALF), BF16), vm((NZ, 16, HALF), BF16), vm((NZ, 16, HALF), BF16),
        vm((16, HALF), BF16), vm((N, 16, COLS), BF16), vm((ROWS, COLS), BF16), vm((ROWS, HD), F32), vm((ROWS, 1), F32),
        pltpu.SemaphoreType.DMA((23,)), pltpu.SemaphoreType.DMA((22,)), pltpu.SemaphoreType.DMA((N,)),
        pltpu.SemaphoreType.DMA((15,)), pltpu.SemaphoreType.DMA((2, NZ)), pltpu.SemaphoreType.DMA((2, NZ)),
        pltpu.SemaphoreType.DMA((4,)),
    ]
    out, nm, nn, nmax = pl.pallas_call(
        layer_kernel,
        out_shape=(
            jax.ShapeDtypeStruct((ROWS, D), BF16),
            jax.ShapeDtypeStruct((ROWS, HD, HD), F32),
            jax.ShapeDtypeStruct((ROWS, HD), F32),
            jax.ShapeDtypeStruct((ROWS, 1), F32),
        ),
        in_specs=[any_] * 23,
        out_specs=(any_,) * 4,
        scratch_shapes=scratch,
        compiler_params=pltpu.CompilerParams(
            collective_id=0, has_side_effects=True, vmem_limit_bytes=60 * 1024 * 1024
        ),
        name="layer",
    )(
        tokens, state_matrix.reshape(ROWS, HD, HD), state_norm.reshape(ROWS, HD), state_max,
        mixer_gain.reshape(1, D), w_query, w_key, w_value, w_outgate, w_ingate, w_forget,
        forget_bias.reshape(1, N), w_proj, ffn_gain.reshape(1, D), w_branch.astype(F32).reshape(1, D), routes,
        route_weight, expert_gate, expert_up, expert_down, dense_gate, dense_up, dense_down,
    )
    return (
        out, nm.reshape(ROWS, 1, HD, HD), nn.reshape(ROWS, 1, HD), nmax,
    )


def solution(mesh):
    in_specs = (
        P("ep", None), P("ep", "tp", None, None), P("ep", "tp", None), P("ep", "tp"), P(),
        P("ep", "tp"), P("ep", "tp"), P("ep", "tp"), P("ep", "tp"), P(), P(), P(), P("tp", "ep"), P(), P(),
        P("ep", None), P("ep", None), P("ep", None, "tp"), P("ep", None, "tp"), P("ep", "tp", None),
        P("ep", "tp"), P("ep", "tp"), P("tp", "ep"),
    )
    out_specs = (P("ep", None), P("ep", "tp", None, None), P("ep", "tp", None), P("ep", "tp"))
    return jax.shard_map(on_device, mesh=mesh, in_specs=in_specs, out_specs=out_specs, check_vma=False)
```

time: 340 us -> 125 us (0.37); the launches traced: 335 us -> 124 us
  waiting for transfers between devices: 168 us -> 0 us
  Pallas kernels: 0 us -> 107 us
  blocking collectives: 48.9 us -> 0 us
  starting transfers between devices: 44.4 us -> 0 us
  matrix products: 20.7 us -> 0 us
  between operations: 14.4 us -> 0.64 us
  other arithmetic: 13.4 us -> 1.3 us
  local copies, waits for them, and re-layouts: 26 us -> 15.2 us
    all_gather x2 -> x0, waiting for transfers between devices: 114 us -> none  [the longest x1 58.5 us: total_of_pieces(): return lax.all_gather(shard, axis).sum(0)]
    pallas_call x0 -> x1, Pallas kernels: none -> 107 us  [on_device(): pl.pallas_call(layer_kernel, out_shape=(jax.ShapeDtypeStruct((ROWS, D), B...]
    all_to_all x7 -> x0, waiting for transfers between devices: 53.7 us -> none  [the longest x3 31 us: sum_at_owner(): lax.all_to_all(parts, axis, split_axis=0, concat_axis=0, tiled=True)]
    all_to_all x4 -> x0, blocking collectives: 48.9 us -> none  [the longest x2 24 us: from_everyone(): lax.all_to_all(jnp.broadcast_to(shard[None], (devices, *shard.shape)), ax...]
    all_to_all x7 -> x0, starting transfers between devices: 44.3 us -> none  [the longest x3 19.2 us: sum_at_owner(): lax.all_to_all(parts, axis, split_axis=0, concat_axis=0, tiled=True)]
    dot_general x14 -> x0, matrix products: 20.7 us -> none  [the longest x4 7.04 us: on_device(): jnp.dot(normed, shard_w, preferred_element_type=jnp.float32)]
    unnamed x36 -> x11, local copies, waits for them, and re-layouts: 0.2 us -> 15.2 us
    scatter x2 -> x0, local copies, waits for them, and re-layouts: 14.8 us -> none  [on_device(): outbound = jnp.zeros((experts_all, capacity, model_width), jnp.bfloat16)....]
  transfers between devices with their start and end apart: 9 -> 0, of which waited for: 7 -> 0; matrix products, arithmetic and copies ran while one was open for 11% -> 0% of each run, Pallas kernels for 0% -> 0%
where the time goes in v1:
time: 125 us; the launch traced here: 124 us
  Pallas kernels  107 us (86%)
  local copies, waits for them, and re-layouts  15.2 us (12%)
  other arithmetic  1.3 us (1%)
    pallas_call x1, Pallas kernels, on_device(): pl.pallas_call(layer_kernel, out_shape=(jax.ShapeDtypeStruct((ROWS, D), B...  107 us
    unnamed x11, local copies, waits for them, and re-layouts  15.2 us

profile of v1, /device:TPU:17, one launch (start us, length us, event | category | flops | bytes accessed | tf_op | source)
XLA Modules:
  0.0 124.4 jit_solution(16343555064385471513)
XLA Ops:
  0.6 1.3 %copy.27.smax_h = f32[32,1]{1,0:T(8,128)} copy(f32[32,1]{0,1:T(1,128)} %param.26) | data formatting | bytes 256 | tf_op args[3]
  2.0 1.3 %reshape.43 = f32[4096]{0:T(1024)} convert(bf16[4096]{0:T(1024)(128)(2,1)} %param.37) | non-fusion elementwise | flops 4096 | bytes 24576 | tf_op jit(solution)/shard_map/reshape | solution.py:525
  3.3 1.4 %copy.30.rt_h = s32[32,2]{1,0:T(8,128)} copy(s32[32,2]{0,1:T(2,128)} %param.38) | data formatting | bytes 512 | tf_op args[15]
  4.6 1.4 %copy.31.rw_h = f32[32,2]{1,0:T(8,128)} copy(f32[32,2]{0,1:T(2,128)} %param.39) | data formatting | bytes 512 | tf_op args[16]
  6.0 2.2 %copy.28.wi_h = bf16[4096,16]{1,0:T(8,128)(2,1)} copy(bf16[4096,16]{0,1:T(8,128)(2,1)} %param.32) | data formatting | bytes 262144 | tf_op args[9]
  8.2 2.2 %copy.29.wf_h = bf16[4096,16]{1,0:T(8,128)(2,1)} copy(bf16[4096,16]{0,1:T(8,128)(2,1)} %param.33) | data formatting | bytes 262144 | tf_op args[10]
  10.5 107.2 %layer.1 = (bf16[32,4096]{1,0:T(8,128)(2,1)}, f32[32,128,128]{2,1,0:T(8,128)}, f32[32,128]{1,0:T(8,128)}, f32[32,1]{1,0:T(8,128)}) custom-call(bf16[32,4096]{1,0:T(8,128)(2,1)} %tok_h.1, f32[32,128,128]{2,1,0:T(8,128)} %bitcast.13, f32[32,128]{1,0:T(8,128)} %bitcast.15, f32[32,1]{1,0:T(8,128)} %copy.27.smax_h, f32[1,4096]{1,0:T(1,128)} %bitcast.16, ...), custom_call_target="tpu_custom_call" | custom-call | tf_op jit(solution)/shard_map/layer/pallas_call | solution.py:507
  117.7 1.3 %copy.34 = f32[32,1]{0,1:T(1,128)} copy(f32[32,1]{1,0:T(8,128)} %get-tuple-element.15) | data formatting | bytes 256
  119.0 1.7 %copy.38 = bf16[32,4096]{1,0:T(8,128)(2,1)} copy(bf16[32,4096]{1,0:T(8,128)(2,1)} %get-tuple-element.20) | data formatting | bytes 524288
  120.7 0.0 copy-start
  120.7 3.1 %copy.39 = f32[32,1,128,128]{3,2,1,0:T(8,128)} copy(f32[32,1,128,128]{3,2,1,0:T(8,128)} %bitcast.12) | data formatting | bytes 4194304
  123.8 0.0 copy-done
  123.8 0.6 copy.40
Async XLA Ops:
  120.7 3.2 %copy-start = (f32[32,128]{1,0:T(8,128)S(1)}, f32[32,128]{1,0:T(8,128)}, u32[]{:S(2)}) copy-start(f32[32,128]{1,0:T(8,128)} %get-tuple-element.10) | copy-start | bytes 49156

commit v2 on v1

v2 whole, which is shorter than its diff:
```python
import functools

import jax
import jax.numpy as jnp
from jax import lax
from jax.experimental import pallas as pl
from jax.experimental.pallas import tpu as pltpu
from jax.sharding import PartitionSpec as P

EPS = 1e-06
MESH = pl.DeviceIdType.MESH
F32 = jnp.float32
BF16 = jnp.bfloat16
N = 16
NZ = 8
ROWS = 32
D = 4096
COLS = 256
HALF = 2048
HD = 128
SECOND_AT = 4


def dot(a, b):
    return jnp.dot(a, b, preferred_element_type=F32)


def dot_rows(a, b):
    return lax.dot_general(a, b, (((1,), (1,)), ((), ())), preferred_element_type=F32)


def layer_kernel(
    tok_h, st_h, sn_h, smax_h, gmix_h, wq_h, wk_h, wv_h, wo_h, wi_h, wf_h, fb_h, wp_h, gffn_h, wbr_h,
    rt_h, rw_h, eg_h, eu_h, ed_h, dg_h, du_h, dd_h,
    out_h, nm_h, nn_h, nmax_h,
    tok, st, sn, smax, gmix, wq, wi, wf, fb, wp, gffn, wbr, rt, rw, eg, eu, ed, dgu, dd,
    xall, csend, crecv, mhall, heads, num,
    wpall, wtab, resall,
    part2, pd2d2, rsend2, rrecv2,
    rtsend, rtall, dsg, dsu, r1g, r1u, d2g, d2u, r2g, r2u, stsend, strecv, hall, r2all, aall,
    xs, xfull, aexp, acc, yp, yd2d, ys, yin, outv, ofull, nnv, nmaxv,
    load_sem, ssem, bsem, rsem, zsem, z2sem, osem, hsem, gsem, store_sem,
):
    e = lax.axis_index("ep")
    t = lax.axis_index("tp")
    z = t // 2
    c = lax.rem(t, 2)
    mate = 2 * z + 1 - c

    def rcopy(src, dst, send, recv, pe, pt):
        return pltpu.make_async_remote_copy(
            src_ref=src, dst_ref=dst, send_sem=send, recv_sem=recv, device_id=(pe, pt), device_id_type=MESH
        )

    def wait_for(ref, sem):
        pltpu.make_async_copy(ref, ref, sem).wait()

    def either(less, ref_less, ref_all, sem):
        @pl.when(less)
        def _():
            wait_for(ref_less, sem)

        @pl.when(jnp.logical_not(less))
        def _():
            wait_for(ref_all, sem)

    def up(d):
        return lax.rem(e + d, N)

    def down(d):
        return lax.rem(e + N - d, N)

    def over_ep(fn):
        lax.fori_loop(1, N, lambda d, carry: (fn(up(d)), carry)[1], 0)

    def over_z(fn):
        lax.fori_loop(1, NZ, lambda d, carry: (fn(lax.rem(z + d, NZ)), carry)[1], 0)

    def cols(index):
        return pl.ds(pl.multiple_of(index * COLS, COLS), COLS)

    def half(index):
        return pl.ds(pl.multiple_of(index * HALF, HALF), HALF)

    scopes = []

    def mark(name):
        if scopes:
            scopes.pop().__exit__(None, None, None)
        if name:
            scopes.append(jax.named_scope(name))
            scopes[-1].__enter__()

    mark("a_barrier")
    loads = [
        (tok_h, tok), (gmix_h, gmix),
        (wq_h, wq.at[:, 0:128]), (wk_h, wq.at[:, 128:256]), (wv_h, wq.at[:, 256:384]), (wo_h, wq.at[:, 384:512]),
        (wi_h, wi), (wf_h, wf), (fb_h, fb), (smax_h, smax), (sn_h, sn), (st_h, st), (wp_h, wp), (gffn_h, gffn),
        (wbr_h, wbr), (rt_h, rt), (rw_h, rw), (dg_h, dgu.at[:, 0:512]), (du_h, dgu.at[:, 512:1024]), (dd_h, dd),
        (eg_h.at[0], eg), (eu_h.at[0], eu), (ed_h.at[0], ed),
    ]
    copies = [pltpu.make_async_copy(s, d, load_sem.at[i]) for i, (s, d) in enumerate(loads)]
    for copy in copies:
        copy.start()

    barrier = pltpu.get_barrier_semaphore()

    def greet_ep(p):
        pl.semaphore_signal(barrier, inc=1, device_id=(p, t), device_id_type=MESH)

    def greet_tp(d, carry):
        pl.semaphore_signal(barrier, inc=1, device_id=(e, lax.rem(t + d, N)), device_id_type=MESH)
        return carry

    over_ep(greet_ep)
    lax.fori_loop(1, N, greet_tp, 0)
    copies[0].wait()
    copies[1].wait()
    pl.semaphore_wait(barrier, 2 * (N - 1))

    mark("b_spread_gates")
    over_ep(lambda p: rcopy(tok.at[:, cols(p)], xall.at[e], ssem.at[0], bsem.at[e], p, t).start())
    copies[12].wait()
    mine_wp = wpall.at[pl.ds(pl.multiple_of(t * HD, HD), HD), :]
    rcopy(wp, mine_wp, ssem.at[4], z2sem.at[2, z], e, mate).start()
    over_z(lambda p: rcopy(wp, mine_wp, ssem.at[5], zsem.at[2, z], e, 2 * p + c).start())
    wpall[pl.ds(pl.multiple_of(t * HD, HD), HD), :] = wp[...]
    xall[e] = tok[:, cols(e)]
    gain_e = gmix[:, cols(e)]

    total = jnp.zeros((ROWS, 128), F32)
    for k in range(8):
        wide = tok[:, k * 512:(k + 1) * 512].astype(F32)
        sq = wide * wide
        total = total + (sq[:, 0:128] + sq[:, 128:256]) + (sq[:, 256:384] + sq[:, 384:512])
    rstd = lax.rsqrt(jnp.sum(total, axis=1, keepdims=True) * (1.0 / D) + EPS)
    for i in (6, 7, 8, 9, 15, 16):
        copies[i].wait()
    gi = jnp.zeros((ROWS, N), F32)
    gf = jnp.zeros((ROWS, N), F32)
    for k in range(8):
        cut = slice(k * 512, (k + 1) * 512)
        nb = (tok[:, cut].astype(F32) * rstd * gmix[:, cut]).astype(BF16)
        gi = gi + dot_rows(nb, wi[:, cut])
        gf = gf + dot_rows(nb, wf[:, cut])
    gf = gf + fb[...]
    mine = lax.broadcasted_iota(jnp.int32, (ROWS, N), 1) == t
    gate_in = jnp.sum(jnp.where(mine, gi, 0.0), axis=1, keepdims=True)
    gate_f = jnp.sum(jnp.where(mine, gf, 0.0), axis=1, keepdims=True)
    log_keep = jnp.minimum(gate_f, 0.0) - jnp.log1p(jnp.exp(-jnp.abs(gate_f)))
    square = lax.broadcasted_iota(jnp.int32, (ROWS, ROWS), 0) == lax.broadcasted_iota(jnp.int32, (ROWS, ROWS), 1)
    kept = log_keep + jnp.sum(jnp.where(square, smax[...], 0.0), axis=1, keepdims=True)
    new_max = jnp.maximum(kept, gate_in)
    keep = jnp.exp(kept - new_max)
    write = jnp.exp(gate_in - new_max)
    nmaxv[...] = jnp.sum(jnp.where(square, new_max, 0.0), axis=0, keepdims=True)
    rtsend[...] = jnp.full((8, 128), -1.0, F32)
    rtsend[0:2, 0:ROWS] = rt[...].astype(F32)
    rtsend[2:4, 0:ROWS] = rw[...]
    over_ep(lambda p: rcopy(rtsend, rtall.at[e], ssem.at[1], rsem.at[0], p, t).start())
    rtall[e] = rtsend[...]
    for i in (2, 3, 4, 5, 10, 11):
        copies[i].wait()

    mark("c_qkvo_part")
    for g in range(4):
        ps = [down(4 * g + j) for j in range(4)]
        for j in range(4):
            if 4 * g + j:
                wait_for(xall.at[ps[j]], bsem.at[ps[j]])
        block = jnp.concatenate([xall[p] for p in ps], axis=0)
        prod = dot((block.astype(F32) * gain_e).astype(BF16), wq[...])
        for j in range(4):
            piece = prod[32 * j:32 * j + 32].astype(BF16)
            if 4 * g + j:
                csend[ps[j]] = piece
                rcopy(csend.at[ps[j]], crecv.at[e], ssem.at[2], rsem.at[1], ps[j], t).start()
            else:
                crecv[e] = piece
    mark("d_wait_qkvo")
    wait_for(crecv.at[0:15], rsem.at[1])
    mark("e_cell")
    qkvo = crecv[0].astype(F32)
    for i in range(1, N):
        qkvo = qkvo + crecv[i].astype(F32)
    qkvo = qkvo * rstd
    q = qkvo[:, 0:128]
    kw = qkvo[:, 128:256] * (HD ** -0.5) * write
    v = qkvo[:, 256:384]
    keep_w = jnp.broadcast_to(keep, (ROWS, HD))
    new_norm = keep_w * sn[...] + kw
    nnv[...] = new_norm
    kw_t = jnp.transpose(kw)
    q_t = jnp.transpose(q)
    for b in range(ROWS):
        new = keep_w[b:b + 1, :] * st[b] + kw_t[:, b:b + 1] * v[b:b + 1, :]
        st[b] = new
        num[b:b + 1, :] = jnp.sum(q_t[:, b:b + 1] * new, axis=0, keepdims=True)
    denom = jnp.maximum(jnp.abs(jnp.sum(q * new_norm, axis=1, keepdims=True)), 1.0)
    mhall[e] = (jax.nn.sigmoid(qkvo[:, 384:512]) * (num[...] / denom)).astype(BF16)
    over_ep(lambda p: rcopy(mhall.at[e], mhall.at[e], ssem.at[23], hsem.at[e], p, t).start())
    head_cols = pl.ds(pl.multiple_of(t * HD, HD), HD)

    def turn_heads(d, carry):
        p = down(d)

        @pl.when(d > 0)
        def _():
            wait_for(mhall.at[p], hsem.at[p])

        @pl.when(p != t)
        def _():
            rcopy(mhall.at[p], heads.at[:, head_cols], ssem.at[3], rsem.at[2], e, p).start()

        @pl.when(p == t)
        def _():
            heads[:, head_cols] = mhall[p]

        return carry

    stores = [
        pltpu.make_async_copy(st, nm_h, store_sem.at[0]),
        pltpu.make_async_copy(nnv, nn_h, store_sem.at[1]),
        pltpu.make_async_copy(nmaxv, nmax_h, store_sem.at[2]),
    ]
    for store in stores:
        store.start()

    mark("f_tables")
    wait_for(rtall.at[0:15], rsem.at[0])
    before = (lax.broadcasted_iota(jnp.int32, (128, 128), 0) < lax.broadcasted_iota(jnp.int32, (128, 128), 1)).astype(BF16)
    row8 = lax.broadcasted_iota(jnp.int32, (128, 128), 0)
    row_e = (row8 // 8).astype(F32)
    row_s = lax.rem(row8, 8).astype(F32)

    def table(group):
        info = rtall[group]
        first = (info[0:1, :] == row_e).astype(F32)
        second = (info[1:2, :] == row_e).astype(F32)
        slot = dot((first + second).astype(BF16), before)
        fits = (slot == row_s).astype(F32)
        share = 1.0 / (info[2:3, :] + info[3:4, :])
        pick = (first + second) * fits
        weigh = (first * (info[2:3, :] * share) + second * (info[3:4, :] * share)) * fits
        return pick[:, 0:ROWS], weigh

    pick0 = table(2 * z)[0]
    pick1 = table(2 * z + 1)[0]

    def wp_rows(index):
        return wpall.at[pl.ds(pl.multiple_of(index * HD, HD), HD), :]

    for d in range(1, NZ):
        p = lax.rem(z + NZ - d, NZ)
        wait_for(wp_rows(2 * p + c), zsem.at[2, p])
        rcopy(wp_rows(2 * p + c), wp_rows(2 * p + c), ssem.at[21], z2sem.at[2, p], e, mate).start()
    lax.fori_loop(0, N, turn_heads, 0)
    mark("g_wait_heads")
    def combine_table(k, carry):
        turned = jnp.transpose(table(2 * k + c)[1])[0:ROWS, :]
        high = turned.astype(BF16)
        wtab[k, 0] = high
        wtab[k, 1] = (turned - high.astype(F32)).astype(BF16)
        return carry

    lax.fori_loop(0, NZ, combine_table, 0)

    for d in range(NZ):
        p = lax.rem(z + NZ - d, NZ)
        wait_for(wp_rows(2 * p + 1 - c), z2sem.at[2, p])

    wait_for(heads.at[:, 0:15 * HD], rsem.at[2])
    mark("h_proj")
    mix = dot(heads[...], wpall[...])
    res_own = (xall[t].astype(F32) + mix).astype(BF16)
    resall[z, c] = res_own

    mark("j_ag_send")
    rcopy(resall.at[z, c], resall.at[z, c], ssem.at[6], z2sem.at[0, z], e, mate).start()
    over_z(lambda p: rcopy(resall.at[z, c], resall.at[z, c], ssem.at[7], zsem.at[0, z], e, 2 * p + c).start())
    mark("k_wait_mate_dispatch")
    wait_for(resall.at[z, 1 - c], z2sem.at[0, z])
    both = jnp.concatenate([resall[z, 0], resall[z, 1]], axis=0)
    zero = jnp.zeros((8, ROWS), F32)
    spread = []
    for ex in range(N):
        spread.append(jnp.concatenate([pick0[8 * ex:8 * ex + 8], zero], axis=1))
        spread.append(jnp.concatenate([zero, pick1[8 * ex:8 * ex + 8]], axis=1))
    routed = dot(jnp.concatenate(spread, axis=0).astype(BF16), both).astype(BF16)
    for ex in range(N):
        xs[ex] = routed[16 * ex:16 * ex + 16]
    over_ep(lambda p: rcopy(xs.at[p], xfull.at[z, :, cols(e)], ssem.at[8], rsem.at[5], p, t).start())
    xfull[z, :, cols(e)] = xs[e]

    for i in (13, 14, 17, 18):
        copies[i].wait()
    mark("l_ag_forward")
    for d in range(1, NZ):
        p = lax.rem(z + NZ - d, NZ)
        wait_for(resall.at[p, c], zsem.at[0, p])
        rcopy(resall.at[p, c], resall.at[p, c], ssem.at[9], z2sem.at[0, p], e, mate).start()

    mark("m_wait_dispatch")
    wait_for(xs.at[0:15], rsem.at[5])
    over_z(lambda p: rcopy(xfull.at[z, :, half(c)], xfull.at[z, :, half(c)], ssem.at[10], zsem.at[1, z], e, 2 * p + c).start())

    mark("n_wait_fwd_dense")
    gain_f = gffn[:, cols(e)]
    sub = lax.broadcasted_iota(jnp.int32, (ROWS, HD), 0)
    w_rows = wbr[...].astype(F32)
    w_b = jnp.concatenate(
        [jnp.sum(jnp.where(sub == 2 * e + k, w_rows, 0.0), axis=0, keepdims=True) for k in range(2)], axis=1
    ).astype(BF16)
    for d in range(1, NZ):
        p = lax.rem(z + NZ - d, NZ)
        wait_for(resall.at[p, 1 - c], z2sem.at[0, p])
    for k in range(NZ):
        wide = jnp.concatenate([resall[k, 0], resall[k, 1]], axis=0).astype(F32)
        r2all[64 * k:64 * k + 64] = (wide * wide).astype(BF16)
        aall[64 * k:64 * k + 64] = (wide * gain_f).astype(BF16)

    def dense_block(g, carry):
        rows = pl.ds(pl.multiple_of(g * 128, 128), 128)
        lhs = aall[rows, :]
        for h in range(2):
            prod = dot(lhs, dgu[:, 512 * h:512 * h + 512])
            for j in range(4):
                piece = prod[32 * j:32 * j + 32].astype(BF16)
                if h == 0:
                    dsg[j, g] = piece
                else:
                    dsu[g, j] = piece
        stat = dot_rows(jnp.ones((8, COLS), BF16), r2all[rows, :])
        br = dot_rows(jnp.broadcast_to(w_b, (8, COLS)), lhs)
        sub = lax.broadcasted_iota(jnp.int32, (8, 128), 0)
        stsend[g] = jnp.where(sub < 4, stat, br)
        return carry

    lax.fori_loop(0, 4, dense_block, 0)
    ey, ex_ = e // 4, lax.rem(e, 4)
    for d in (2, 1, 3):
        px, py = lax.rem(ex_ + d, 4), lax.rem(ey + d, 4)
        rcopy(dsg.at[px], r1g.at[ex_], ssem.at[11], gsem.at[0], 4 * ey + px, t).start()
        rcopy(dsu.at[py], r1u.at[ey], ssem.at[24], gsem.at[1], 4 * py + ex_, t).start()
    over_ep(lambda p: rcopy(stsend.at[p // 4], strecv.at[e], ssem.at[12], rsem.at[7], p, t).start())
    r1g[ex_] = dsg[ex_]
    r1u[ey] = dsu[ey]
    strecv[e] = stsend[e // 4]

    mark("o_expert_fwd")
    def second_stage():
        for parts, got, mine, left, sem in ((r1g, d2g, ey, r2g, 0), (r1u, d2u, ex_, r2u, 1)):
            wait_for(parts.at[0:3], gsem.at[sem])
            for k in range(4):
                tot = parts[0, k].astype(F32) + parts[1, k].astype(F32)
                got[k] = (tot + parts[2, k].astype(F32) + parts[3, k].astype(F32)).astype(BF16)
            left[mine] = got[mine]
            for d in (2, 1, 3):
                other = lax.rem(mine + d, 4)
                target = 4 * other + ex_ if sem == 0 else 4 * ey + other
                rcopy(got.at[other], left.at[mine], ssem.at[25 + sem], gsem.at[2 + sem], target, t).start()

    for d in range(1, NZ):
        p = lax.rem(z + NZ - d, NZ)
        wait_for(xfull.at[p, :, half(c)], zsem.at[1, p])
        rcopy(xfull.at[p, :, half(c)], xfull.at[p, :, half(c)], ssem.at[13], z2sem.at[1, p], e, mate).start()
        if d == SECOND_AT:
            second_stage()

    mark("p_wait_dense")
    wait_for(r2g.at[0:3], gsem.at[2])
    wait_for(r2u.at[0:3], gsem.at[3])
    wait_for(strecv.at[0:15], rsem.at[7])
    mark("q_hidden")
    stats = strecv[0]
    for i in range(1, N):
        stats = stats + strecv[i]
    lane = lax.broadcasted_iota(jnp.int32, (ROWS, 128), 1)
    at = lane == lax.broadcasted_iota(jnp.int32, (ROWS, 128), 0) + ROWS * lax.rem(e, 4)
    sumsq = jnp.sum(jnp.where(at, stats[0:1, :], 0.0), axis=1, keepdims=True)
    branch = jnp.sum(jnp.where(at, stats[4:5, :], 0.0), axis=1, keepdims=True)
    rstd2 = lax.rsqrt(sumsq * (1.0 / D) + EPS)
    branch_share = jax.nn.sigmoid(branch * rstd2)
    for h in range(2):
        cg = slice(256 * h, 256 * h + 256)
        g_ = r2g[0, :, cg].astype(F32)
        u_ = r2u[0, :, cg].astype(F32)
        for i in range(1, 4):
            g_ = g_ + r2g[i, :, cg].astype(F32)
            u_ = u_ + r2u[i, :, cg].astype(F32)
        g_ = g_ * rstd2
        u_ = u_ * rstd2
        hall[e, :, cg] = (g_ * jax.nn.sigmoid(g_) * u_ * branch_share).astype(BF16)
    over_ep(lambda p: rcopy(hall.at[e], hall.at[e], ssem.at[14], rsem.at[8], p, t).start())

    mark("r_wait_expert")
    for i in (20, 21, 22):
        copies[i].wait()
    for d in range(1, NZ):
        p = lax.rem(z + NZ - d, NZ)
        wait_for(xfull.at[p, :, half(1 - c)], z2sem.at[1, p])

    mark("s_expert")
    def expert_rows(k, carry):
        tot = jnp.zeros((16, 128), F32)
        for m in range(4):
            wide = xfull[k, :, 1024 * m:1024 * m + 1024].astype(F32)
            sq = wide * wide
            for n in range(8):
                tot = tot + sq[:, 128 * n:128 * n + 128]
        scale = lax.rsqrt(jnp.sum(tot, axis=1, keepdims=True) * (1.0 / D) + EPS)
        rows = pl.ds(pl.multiple_of(k * 16, 16), 16)
        for m in range(4):
            cut = slice(1024 * m, 1024 * m + 1024)
            aexp[rows, cut] = (xfull[k, :, cut].astype(F32) * scale * gffn[:, cut]).astype(BF16)
        return carry

    lax.fori_loop(0, NZ, expert_rows, 0)
    acc[...] = jnp.zeros_like(acc)

    def expert_in(k, carry):
        cut = pl.ds(pl.multiple_of(k * 512, 512), 512)
        lhs = aexp[:, cut]
        acc[:, 0:256] += dot(lhs, eg[cut, :])
        acc[:, 256:512] += dot(lhs, eu[cut, :])
        return carry

    lax.fori_loop(0, 8, expert_in, 0)
    g_ = acc[:, 0:256]
    hid = (g_ * jax.nn.sigmoid(g_) * acc[:, 256:512]).astype(BF16)
    aexp[:, 0:256] = hid

    def expert_out(k, carry):
        cut = pl.ds(pl.multiple_of(k * 512, 512), 512)
        prod = dot(aexp[:, 0:256], ed[:, cut]).astype(BF16)
        for n in range(NZ):
            yp[n, :, cut] = prod[16 * n:16 * n + 16]
        return carry

    lax.fori_loop(4 * (1 - c), 4 * (1 - c) + 4, expert_out, 0)
    rcopy(yp.at[:, :, half(1 - c)], yd2d, ssem.at[15], rsem.at[9], e, mate).start()
    lax.fori_loop(4 * c, 4 * c + 4, expert_out, 0)

    mark("r2_pair_sum")
    wait_for(yd2d, rsem.at[9])

    def sum_pair(k, carry):
        both_sum = yp[k, :, half(c)].astype(F32) + yd2d[k].astype(F32)
        ys[0, k] = both_sum[0:8].astype(BF16)
        ys[1, k] = both_sum[8:16].astype(BF16)
        return carry

    lax.fori_loop(0, NZ, sum_pair, 0)

    def back(d, carry):
        j = lax.rem(d + e, NZ)
        pe = c * NZ + j
        rcopy(ys.at[1 - c, :, :, cols(j)], yin.at[:, e], ssem.at[18], rsem.at[12], pe, mate).start()

        @pl.when(pe != e)
        def _():
            rcopy(ys.at[c, :, :, cols(j)], yin.at[:, e], ssem.at[19], rsem.at[12], pe, t).start()

        @pl.when(pe == e)
        def _():
            yin[:, e] = ys[c, :, :, cols(j)]

        return carry

    lax.fori_loop(0, NZ, back, 0)

    mark("t_wait_hidden")
    copies[19].wait()
    wait_for(hall.at[0:15], rsem.at[8])
    mark("u_down")

    def dense_down(g, carry):
        block = jnp.concatenate([hall[4 * g + j] for j in range(4)], axis=0)
        prod = dot(block, dd[...])
        for j in range(4):
            part2[2 * g + j // 2, j % 2] = prod[32 * j:32 * j + 32].astype(BF16)
        return carry

    lax.fori_loop(0, 4, dense_down, 0)
    rcopy(part2.at[:, 1 - c], pd2d2, ssem.at[16], rsem.at[10], e, mate).start()
    mark("v_wait_back")
    either(e // NZ == c, yin.at[:, 0:15], yin, rsem.at[12])
    wait_for(pd2d2, rsem.at[10])
    mark("w_combine")

    def combine(k, carry):
        rows = yin[k].astype(F32).reshape(128, COLS).astype(BF16)
        tot = dot(wtab[k, 0], rows) + dot(wtab[k, 1], rows)
        rsend2[k] = (tot + part2[k, c].astype(F32) + pd2d2[k].astype(F32)).astype(BF16)
        return carry

    lax.fori_loop(0, NZ, combine, 0)
    over_z(lambda p: rcopy(rsend2.at[p], rrecv2.at[z], ssem.at[17], rsem.at[11], e, 2 * p + c).start())
    rrecv2[z] = rsend2[z]
    mark("x_wait_rs")
    wait_for(rrecv2.at[0:7], rsem.at[11])
    tot = resall[z, c].astype(F32)
    for k in range(NZ):
        tot = tot + rrecv2[k].astype(F32)
    outv[...] = tot.astype(BF16)

    mark("z_deliver")
    def deliver(d, carry):
        p = lax.rem(z + d, NZ)

        @pl.when(jnp.logical_or(t != e, p != z))
        def _():
            rcopy(outv, ofull.at[e], ssem.at[20], osem.at[e], t, 2 * p + c).start()

        return carry

    lax.fori_loop(0, NZ, deliver, 0)

    @pl.when(t == e)
    def _():
        ofull[e] = outv[...]

    first = c == lax.rem(e, 2)

    @pl.when(first)
    def _():
        def pass_on(d, carry):
            p = down(d)

            @pl.when(jnp.logical_or(t != e, p != e))
            def _():
                wait_for(ofull.at[p], osem.at[p])

            rcopy(ofull.at[p], out_h.at[:, cols(p)], ssem.at[22], rsem.at[14], e, mate).start()
            pltpu.make_async_copy(ofull.at[p], out_h.at[:, cols(p)], store_sem.at[3]).start()
            return carry

        lax.fori_loop(0, N, pass_on, 0)
        wait_for(ofull, store_sem.at[3])
        wait_for(ofull, ssem.at[22])

    @pl.when(jnp.logical_not(first))
    def _():
        wait_for(out_h, rsem.at[14])

    mark("zz_end")
    wait_for(xall.at[0:15], ssem.at[0])
    wait_for(rtall.at[0:15], ssem.at[1])
    wait_for(csend.at[0:15], ssem.at[2])
    wait_for(heads.at[:, 0:15 * HD], ssem.at[3])
    wait_for(mhall.at[0:15], ssem.at[23])
    wait_for(wp, ssem.at[4])
    wait_for(wpall.at[0:7 * HD], ssem.at[5])
    wait_for(resall.at[0, 0], ssem.at[6])
    wait_for(rsend2.at[0:7], ssem.at[7])
    wait_for(xs.at[0:15], ssem.at[8])
    wait_for(rsend2.at[0:7], ssem.at[9])
    wait_for(yd2d.at[0:7], ssem.at[10])
    for i, ref in ((11, dsg), (24, dsu), (25, d2g), (26, d2u)):
        wait_for(ref.at[0:3], ssem.at[i])
    wait_for(strecv.at[0:15], ssem.at[12])
    wait_for(yd2d.at[0:7], ssem.at[13])
    wait_for(hall.at[0:15], ssem.at[14])
    wait_for(yd2d, ssem.at[15])
    wait_for(pd2d2, ssem.at[16])
    wait_for(rsend2.at[0:7], ssem.at[17])
    wait_for(yin.at[:, 0:8], ssem.at[18])
    either(e // NZ == c, yin.at[:, 0:7], yin.at[:, 0:8], ssem.at[19])
    either(t == e, rsend2.at[0:7], rsend2, ssem.at[20])
    wait_for(wpall.at[0:7 * HD], ssem.at[21])
    for store in stores:
        store.wait()
    mark(None)


def finish_kernel(out_a, nm_a, nn_a, nmax_a, out_o, nm_o, nn_o, nmax_o, out_v, nm_v, nn_v, nmax_v, in_sem, out_sem):
    trips = [(nm_a.at[8 * k:8 * k + 8], nm_v.at[8 * k:8 * k + 8], nm_o.at[8 * k:8 * k + 8]) for k in range(4)]
    trips += [(out_a, out_v, out_o), (nn_a, nn_v, nn_o), (nmax_a, nmax_v, nmax_o)]
    ins = [pltpu.make_async_copy(a, v, in_sem.at[i]) for i, (a, v, _) in enumerate(trips)]
    outs = [pltpu.make_async_copy(v, o, out_sem.at[i]) for i, (_, v, o) in enumerate(trips)]
    for copy in ins:
        copy.start()
    for got, put in zip(ins, outs):
        got.wait()
        put.start()
    for put in outs:
        put.wait()


def on_device(
    tokens, state_matrix, state_norm, state_max, mixer_gain, w_query, w_key, w_value, w_outgate, w_ingate, w_forget,
    forget_bias, w_proj, ffn_gain, w_branch, routes, route_weight, expert_gate, expert_up, expert_down,
    dense_gate, dense_up, dense_down,
):
    any_ = pl.BlockSpec(memory_space=pl.ANY)
    vm = pltpu.VMEM
    scratch = [
        vm((ROWS, D), BF16), vm((ROWS, HD, HD), F32), vm((ROWS, HD), F32), vm((1, ROWS), F32), vm((1, D), F32),
        vm((COLS, 512), BF16), vm((N, D), BF16), vm((N, D), BF16), vm((1, N), F32), vm((HD, COLS), BF16),
        vm((1, D), F32), vm((ROWS, HD), BF16), vm((2, ROWS), jnp.int32), vm((2, ROWS), F32),
        vm((D, COLS), BF16), vm((D, COLS), BF16), vm((COLS, D), BF16), vm((COLS, 1024), BF16), vm((512, COLS), BF16),
        vm((N, ROWS, COLS), BF16), vm((N, ROWS, 512), BF16), vm((N, ROWS, 512), BF16), vm((N, ROWS, HD), BF16),
        vm((ROWS, HALF), BF16), vm((ROWS, HD), F32),
        vm((HALF, COLS), BF16), vm((NZ, 2, ROWS, HD), BF16), vm((NZ, 2, ROWS, COLS), BF16),
        vm((NZ, 2, ROWS, COLS), BF16), vm((NZ, ROWS, COLS), BF16), vm((NZ, ROWS, COLS), BF16),
        vm((NZ, ROWS, COLS), BF16),
        vm((8, 128), F32), vm((N, 8, 128), F32),
        vm((4, 4, ROWS, 512), BF16), vm((4, 4, ROWS, 512), BF16), vm((4, 4, ROWS, 512), BF16),
        vm((4, 4, ROWS, 512), BF16), vm((4, ROWS, 512), BF16), vm((4, ROWS, 512), BF16), vm((4, ROWS, 512), BF16),
        vm((4, ROWS, 512), BF16),
        vm((4, 8, 128), F32), vm((N, 8, 128), F32), vm((N, ROWS, 512), BF16), vm((512, COLS), BF16),
        vm((512, COLS), BF16),
        vm((N, 16, COLS), BF16), vm((NZ, 16, D), BF16), vm((128, D), BF16), vm((128, 512), F32),
        vm((NZ, 16, D), BF16), vm((NZ, 16, HALF), BF16), vm((2, NZ, 8, HALF), BF16), vm((NZ, N, 8, COLS), BF16),
        vm((ROWS, COLS), BF16), vm((N, ROWS, COLS), BF16), vm((ROWS, HD), F32), vm((1, ROWS), F32),
        pltpu.SemaphoreType.DMA((23,)), pltpu.SemaphoreType.DMA((27,)), pltpu.SemaphoreType.DMA((N,)),
        pltpu.SemaphoreType.DMA((15,)), pltpu.SemaphoreType.DMA((3, NZ)), pltpu.SemaphoreType.DMA((3, NZ)),
        pltpu.SemaphoreType.DMA((N,)), pltpu.SemaphoreType.DMA((N,)), pltpu.SemaphoreType.DMA((4,)),
        pltpu.SemaphoreType.DMA((4,)),
    ]
    shapes = (
        jax.ShapeDtypeStruct((ROWS, D), BF16),
        jax.ShapeDtypeStruct((ROWS, HD, HD), F32),
        jax.ShapeDtypeStruct((ROWS, HD), F32),
        jax.ShapeDtypeStruct((1, ROWS), F32),
    )
    results = pl.pallas_call(
        layer_kernel,
        out_shape=shapes,
        in_specs=[any_] * 23,
        out_specs=(any_,) * 4,
        scratch_shapes=scratch,
        compiler_params=pltpu.CompilerParams(
            collective_id=0, has_side_effects=True, vmem_limit_bytes=60 * 1024 * 1024
        ),
        name="layer",
    )(
        tokens, state_matrix.reshape(ROWS, HD, HD), state_norm.reshape(ROWS, HD), state_max.T,
        mixer_gain.reshape(1, D), w_query, w_key, w_value, w_outgate, w_ingate.T, w_forget.T,
        forget_bias.reshape(1, N), w_proj, ffn_gain.reshape(1, D), w_branch.reshape(ROWS, HD), routes.T,
        route_weight.T, expert_gate, expert_up, expert_down, dense_gate, dense_up, dense_down,
    )
    out, nm, nn, nmax = pl.pallas_call(
        finish_kernel,
        out_shape=shapes,
        in_specs=[any_] * 4,
        out_specs=(any_,) * 4,
        scratch_shapes=[vm(shape.shape, shape.dtype) for shape in shapes]
        + [pltpu.SemaphoreType.DMA((7,)), pltpu.SemaphoreType.DMA((7,))],
        name="finish",
    )(*results)
    return (
        out, nm.reshape(ROWS, 1, HD, HD), nn.reshape(ROWS, 1, HD), nmax.T,
    )


def solution(mesh):
    in_specs = (
        P("ep", None), P("ep", "tp", None, None), P("ep", "tp", None), P("ep", "tp"), P(),
        P("ep", "tp"), P("ep", "tp"), P("ep", "tp"), P("ep", "tp"), P(), P(), P(), P("tp", "ep"), P(), P(),
        P("ep", None), P("ep", None), P("ep", None, "tp"), P("ep", None, "tp"), P("ep", "tp", None),
        P("ep", "tp"), P("ep", "tp"), P("tp", "ep"),
    )
    out_specs = (P("ep", None), P("ep", "tp", None, None), P("ep", "tp", None), P("ep", "tp"))
    return jax.shard_map(on_device, mesh=mesh, in_specs=in_specs, out_specs=out_specs, check_vma=False)
```

time: 125 us -> 95.1 us (0.76)
  local copies, waits for them, and re-layouts: 15.2 us -> 0 us
  Pallas kernels: 107 us -> 94.4 us
  other arithmetic: 1.3 us -> 0 us
    unnamed x11 -> x0, local copies, waits for them, and re-layouts: 15.2 us -> none
    pallas_call x1 -> x2, Pallas kernels: 107 us -> 94.4 us  [the longest x1 91.8 us: on_device(): pl.pallas_call(layer_kernel, out_shape=shapes, in_specs=[any_] * 23, out_...]
    reshape x1 -> x0, other arithmetic: 1.3 us -> none  [on_device(): w_branch.astype(F32).reshape(1, D)]
where the time goes in v2:
time: 95.1 us; the launch traced here: 95 us
  Pallas kernels  94.4 us (99%)
    pallas_call x1, Pallas kernels, on_device(): pl.pallas_call(layer_kernel, out_shape=shapes, in_specs=[any_] * 23, out_...  91.8 us
    pallas_call x1, Pallas kernels, on_device(): pl.pallas_call(finish_kernel, out_shape=shapes, in_specs=[any_] * 4, out_...  2.56 us

profile of v2, /device:TPU:17, one launch (start us, length us, event | category | flops | bytes accessed | tf_op | source)
XLA Modules:
  0.0 95.0 jit_solution(11807756114544870801)
XLA Ops:
  0.6 91.8 %layer.1 = (bf16[32,4096]{1,0:T(8,128)(2,1)}, f32[32,128,128]{2,1,0:T(8,128)}, f32[32,128]{1,0:T(8,128)}, f32[1,32]{1,0:T(1,128)}) custom-call(bf16[32,4096]{1,0:T(8,128)(2,1)} %tok_h.1, f32[32,128,128]{2,1,0:T(8,128)} %bitcast.18, f32[32,128]{1,0:T(8,128)} %bitcast.21, f32[1,32]{1,0:T(1,128)} %bitcast.27, f32[1,4096]{1,0:T(1,128)} %bitcast.22, ...), custom_call_target="tpu_custom_call" | custom-call | tf_op jit(solution)/shard_map/layer/pallas_call | solution.py:627
  92.4 2.6 %finish.1 = (bf16[32,4096]{1,0:T(8,128)(2,1)}, f32[32,128,128]{2,1,0:T(8,128)}, f32[32,128]{1,0:T(8,128)}, f32[1,32]{1,0:T(1,128)}) custom-call(bf16[32,4096]{1,0:T(8,128)(2,1)} %get-tuple-element.12.out_a, f32[32,128,128]{2,1,0:T(8,128)} %get-tuple-element.13.nm_a, f32[32,128]{1,0:T(8,128)} %get-tuple-element.14.nn_a, f32[1,32]{1,0:T(1,128)} %get-tuple-element.15.nmax_a), custom_call_target="tpu_custom_call" | custom-call | tf_op jit(solution)/shard_map/finish/pallas_call | solution.py:643

commit v3 on v2

--- a/solution.py
+++ b/solution.py
@@ -18,7 +18,12 @@
 COLS = 256
 HALF = 2048
 HD = 128
-SECOND_AT = 4
+SECOND_AT = 1
+HOPS = (0, 1, 2, 1)
+EP_ORDER = sorted(
+    [(dy, dx) for dy in range(4) for dx in range(4) if dy + dx], key=lambda o: -(HOPS[o[0]] + HOPS[o[1]])
+)
+Z_ORDER = (4, 3, 5, 2, 6, 1, 7)
 
 
 def dot(a, b):
@@ -37,15 +42,16 @@
     xall, csend, crecv, mhall, heads, num,
     wpall, wtab, resall,
     part2, pd2d2, rsend2, rrecv2,
-    rtsend, rtall, dsg, dsu, r1g, r1u, d2g, d2u, r2g, r2u, stsend, strecv, hall, r2all, aall,
-    xs, xfull, aexp, acc, yp, yd2d, ys, yin, outv, ofull, nnv, nmaxv,
-    load_sem, ssem, bsem, rsem, zsem, z2sem, osem, hsem, gsem, store_sem,
+    rtsend, rtall, dsg, dsu, r1g, r1u, d2g, d2u, r2g, r2u, stsend, strecv, halla, hallb, r2all, aall,
+    xsa, xsb, xfa, xfb, aexp, acc, yp, yd2d, ys, yin, outv, ofull, nnv, nmaxv,
+    load_sem, ssem, bsem, rsem, zsem, z2sem, osem, hsem, gsem, dsem, lsem, store_sem,
 ):
     e = lax.axis_index("ep")
     t = lax.axis_index("tp")
     z = t // 2
     c = lax.rem(t, 2)
     mate = 2 * z + 1 - c
+    ey, ex_ = e // 4, lax.rem(e, 4)
 
     def rcopy(src, dst, send, recv, pe, pt):
         return pltpu.make_async_remote_copy(
@@ -64,17 +70,22 @@
         def _():
             wait_for(ref_all, sem)
 
-    def up(d):
-        return lax.rem(e + d, N)
+    def ahead(offset):
+        return 4 * lax.rem(ey + offset[0], 4) + lax.rem(ex_ + offset[1], 4)
+
+    def behind(offset):
+        return 4 * lax.rem(ey + 4 - offset[0], 4) + lax.rem(ex_ + 4 - offset[1], 4)
 
     def down(d):
         return lax.rem(e + N - d, N)
 
     def over_ep(fn):
-        lax.fori_loop(1, N, lambda d, carry: (fn(up(d)), carry)[1], 0)
+        for offset in EP_ORDER:
+            fn(ahead(offset))
 
     def over_z(fn):
-        lax.fori_loop(1, NZ, lambda d, carry: (fn(lax.rem(z + d, NZ)), carry)[1], 0)
+        for d in Z_ORDER:
+            fn(lax.rem(z + d, NZ))
 
     def cols(index):
         return pl.ds(pl.multiple_of(index * COLS, COLS), COLS)
@@ -164,7 +175,7 @@
 
     mark("c_qkvo_part")
     for g in range(4):
-        ps = [down(4 * g + j) for j in range(4)]
+        ps = [e if 4 * g + j == 0 else behind(EP_ORDER[4 * g + j - 1]) for j in range(4)]
         for j in range(4):
             if 4 * g + j:
                 wait_for(xall.at[ps[j]], bsem.at[ps[j]])
@@ -201,13 +212,7 @@
     over_ep(lambda p: rcopy(mhall.at[e], mhall.at[e], ssem.at[23], hsem.at[e], p, t).start())
     head_cols = pl.ds(pl.multiple_of(t * HD, HD), HD)
 
-    def turn_heads(d, carry):
-        p = down(d)
-
-        @pl.when(d > 0)
-        def _():
-            wait_for(mhall.at[p], hsem.at[p])
-
+    def turn_heads(p):
         @pl.when(p != t)
         def _():
             rcopy(mhall.at[p], heads.at[:, head_cols], ssem.at[3], rsem.at[2], e, p).start()
@@ -215,8 +220,6 @@
         @pl.when(p == t)
         def _():
             heads[:, head_cols] = mhall[p]
-
-        return carry
 
     stores = [
         pltpu.make_async_copy(st, nm_h, store_sem.at[0]),
@@ -231,6 +234,18 @@
     before = (lax.broadcasted_iota(jnp.int32, (128, 128), 0) < lax.broadcasted_iota(jnp.int32, (128, 128), 1)).astype(BF16)
     row8 = lax.broadcasted_iota(jnp.int32, (128, 128), 0)
     row_e = (row8 // 8).astype(F32)
+    row16 = lax.broadcasted_iota(jnp.int32, (256, 128), 0)
+    row16_e = (row16 // 16).astype(F32)
+    row16_q = lax.rem(row16, 16)
+
+    def pick_table(group, low):
+        info = rtall[group]
+        hit = jnp.logical_or(info[0:1, :] == row16_e, info[1:2, :] == row16_e).astype(F32)
+        slot = dot(hit.astype(BF16), before)
+        inside = jnp.logical_and(row16_q >= low, row16_q < low + 6)
+        fits = jnp.logical_and(slot == (row16_q - low).astype(F32), inside).astype(F32)
+        return (hit * fits)[:, 0:ROWS].astype(BF16)
+
     row_s = lax.rem(row8, 8).astype(F32)
 
     def table(group):
@@ -240,30 +255,45 @@
         slot = dot((first + second).astype(BF16), before)
         fits = (slot == row_s).astype(F32)
         share = 1.0 / (info[2:3, :] + info[3:4, :])
-        pick = (first + second) * fits
         weigh = (first * (info[2:3, :] * share) + second * (info[3:4, :] * share)) * fits
-        return pick[:, 0:ROWS], weigh
-
-    pick0 = table(2 * z)[0]
-    pick1 = table(2 * z + 1)[0]
+        return weigh
+
+    pick0 = pick_table(2 * z, 0)
+    pick1 = pick_table(2 * z + 1, 6)
 
     def wp_rows(index):
         return wpall.at[pl.ds(pl.multiple_of(index * HD, HD), HD), :]
 
-    for d in range(1, NZ):
+    for d in Z_ORDER:
         p = lax.rem(z + NZ - d, NZ)
         wait_for(wp_rows(2 * p + c), zsem.at[2, p])
         rcopy(wp_rows(2 * p + c), wp_rows(2 * p + c), ssem.at[21], z2sem.at[2, p], e, mate).start()
-    lax.fori_loop(0, N, turn_heads, 0)
+    turn_heads(e)
+    for offset in EP_ORDER:
+        p = behind(offset)
+        wait_for(mhall.at[p], hsem.at[p])
+        turn_heads(p)
     mark("g_wait_heads")
     def combine_table(k, carry):
-        turned = jnp.transpose(table(2 * k + c)[1])[0:ROWS, :]
+        turned = jnp.transpose(table(2 * k + c))[0:ROWS, :]
         high = turned.astype(BF16)
-        wtab[k, 0] = high
-        wtab[k, 1] = (turned - high.astype(F32)).astype(BF16)
+        low = (turned - high.astype(F32)).astype(BF16)
+        m = lax.rem(k, 4)
+        r = lax.broadcasted_iota(jnp.int32, (128, 384), 0)
+        q = lax.broadcasted_iota(jnp.int32, (128, 384), 1)
+        same = jnp.logical_and(r // 8 == q // 24, lax.rem(q, 24) == 6 * m + lax.rem(r, 8))
+        move = jnp.logical_and(same, lax.rem(r, 8) < 6).astype(F32).astype(BF16)
+        moved = dot(jnp.concatenate([high, low], axis=0), move).astype(BF16)
+        rows = pl.ds(pl.multiple_of(m * ROWS, ROWS), ROWS)
+        wtab[k // 4, 0, rows, :] = moved[0:ROWS]
+        wtab[k // 4, 1, rows, :] = moved[ROWS:2 * ROWS]
         return carry
 
     lax.fori_loop(0, NZ, combine_table, 0)
+    rr = lax.broadcasted_iota(jnp.int32, (96, 128), 0)
+    rq = lax.broadcasted_iota(jnp.int32, (96, 128), 1)
+    rest = lax.rem(rr, 48)
+    keep_rows = (rq == 16 * (rest // 6) + lax.rem(rest, 6) + 6 * (rr // 48)).astype(F32).astype(BF16)
 
     for d in range(NZ):
         p = lax.rem(z + NZ - d, NZ)
@@ -280,68 +310,82 @@
     over_z(lambda p: rcopy(resall.at[z, c], resall.at[z, c], ssem.at[7], zsem.at[0, z], e, 2 * p + c).start())
     mark("k_wait_mate_dispatch")
     wait_for(resall.at[z, 1 - c], z2sem.at[0, z])
-    both = jnp.concatenate([resall[z, 0], resall[z, 1]], axis=0)
-    zero = jnp.zeros((8, ROWS), F32)
-    spread = []
+    routed = dot(pick0, resall[z, 0]) + dot(pick1, resall[z, 1])
     for ex in range(N):
-        spread.append(jnp.concatenate([pick0[8 * ex:8 * ex + 8], zero], axis=1))
-        spread.append(jnp.concatenate([zero, pick1[8 * ex:8 * ex + 8]], axis=1))
-    routed = dot(jnp.concatenate(spread, axis=0).astype(BF16), both).astype(BF16)
-    for ex in range(N):
-        xs[ex] = routed[16 * ex:16 * ex + 16]
-    over_ep(lambda p: rcopy(xs.at[p], xfull.at[z, :, cols(e)], ssem.at[8], rsem.at[5], p, t).start())
-    xfull[z, :, cols(e)] = xs[e]
+        xsa[ex] = routed[16 * ex:16 * ex + 8].astype(BF16)
+        xsb[ex] = routed[16 * ex + 8:16 * ex + 12].astype(BF16)
+    over_ep(lambda p: rcopy(xsa.at[p], xfa.at[z, :, cols(e)], ssem.at[8], rsem.at[5], p, t).start())
+    over_ep(lambda p: rcopy(xsb.at[p], xfb.at[z, :, cols(e)], ssem.at[27], rsem.at[15], p, t).start())
+    xfa[z, :, cols(e)] = xsa[e]
+    xfb[z, :, cols(e)] = xsb[e]
 
     for i in (13, 14, 17, 18):
         copies[i].wait()
     mark("l_ag_forward")
-    for d in range(1, NZ):
-        p = lax.rem(z + NZ - d, NZ)
-        wait_for(resall.at[p, c], zsem.at[0, p])
-        rcopy(resall.at[p, c], resall.at[p, c], ssem.at[9], z2sem.at[0, p], e, mate).start()
-
-    mark("m_wait_dispatch")
-    wait_for(xs.at[0:15], rsem.at[5])
-    over_z(lambda p: rcopy(xfull.at[z, :, half(c)], xfull.at[z, :, half(c)], ssem.at[10], zsem.at[1, z], e, 2 * p + c).start())
-
-    mark("n_wait_fwd_dense")
     gain_f = gffn[:, cols(e)]
     sub = lax.broadcasted_iota(jnp.int32, (ROWS, HD), 0)
     w_rows = wbr[...].astype(F32)
     w_b = jnp.concatenate(
         [jnp.sum(jnp.where(sub == 2 * e + k, w_rows, 0.0), axis=0, keepdims=True) for k in range(2)], axis=1
     ).astype(BF16)
-    for d in range(1, NZ):
+
+    for d in Z_ORDER:
+        p = lax.rem(z + NZ - d, NZ)
+        wait_for(resall.at[p, c], zsem.at[0, p])
+        rcopy(resall.at[p, c], resall.at[p, c], ssem.at[9], z2sem.at[0, p], e, mate).start()
+
+    mark("n_wait_fwd_dense")
+    for d in Z_ORDER:
         p = lax.rem(z + NZ - d, NZ)
         wait_for(resall.at[p, 1 - c], z2sem.at[0, p])
     for k in range(NZ):
         wide = jnp.concatenate([resall[k, 0], resall[k, 1]], axis=0).astype(F32)
         r2all[64 * k:64 * k + 64] = (wide * wide).astype(BF16)
         aall[64 * k:64 * k + 64] = (wide * gain_f).astype(BF16)
-
-    def dense_block(g, carry):
+    def dense_up(i, carry):
+        g = lax.rem(ey + 1 + i, 4)
         rows = pl.ds(pl.multiple_of(g * 128, 128), 128)
-        lhs = aall[rows, :]
-        for h in range(2):
-            prod = dot(lhs, dgu[:, 512 * h:512 * h + 512])
-            for j in range(4):
-                piece = prod[32 * j:32 * j + 32].astype(BF16)
-                if h == 0:
-                    dsg[j, g] = piece
-                else:
-                    dsu[g, j] = piece
+        prod = dot(aall[rows, :], dgu[:, 512:1024])
+        for j in range(4):
+            dsu[g, j] = prod[32 * j:32 * j + 32].astype(BF16)
+
+        @pl.when(g != ey)
+        def _():
+            rcopy(dsu.at[g], r1u.at[ey], ssem.at[24], gsem.at[1], 4 * g + ex_, t).start()
+
+        return carry
+
+    def dense_gate(g, carry):
+        rows = pl.ds(pl.multiple_of(g * 128, 128), 128)
+        prod = dot(aall[rows, :], dgu[:, 0:512])
+        for j in range(4):
+            dsg[j, g] = prod[32 * j:32 * j + 32].astype(BF16)
+        return carry
+
+    def dense_stats(g, carry):
+        rows = pl.ds(pl.multiple_of(g * 128, 128), 128)
         stat = dot_rows(jnp.ones((8, COLS), BF16), r2all[rows, :])
-        br = dot_rows(jnp.broadcast_to(w_b, (8, COLS)), lhs)
-        sub = lax.broadcasted_iota(jnp.int32, (8, 128), 0)
-        stsend[g] = jnp.where(sub < 4, stat, br)
-        return carry
-
-    lax.fori_loop(0, 4, dense_block, 0)
-    ey, ex_ = e // 4, lax.rem(e, 4)
+        br = dot_rows(jnp.broadcast_to(w_b, (8, COLS)), aall[rows, :])
+        sub8 = lax.broadcasted_iota(jnp.int32, (8, 128), 0)
+        stsend[g] = jnp.where(sub8 < 4, stat, br)
+        return carry
+
+    lax.fori_loop(0, 4, dense_up, 0)
+    lax.fori_loop(0, 4, dense_gate, 0)
     for d in (2, 1, 3):
-        px, py = lax.rem(ex_ + d, 4), lax.rem(ey + d, 4)
+        px = lax.rem(ex_ + d, 4)
         rcopy(dsg.at[px], r1g.at[ex_], ssem.at[11], gsem.at[0], 4 * ey + px, t).start()
-        rcopy(dsu.at[py], r1u.at[ey], ssem.at[24], gsem.at[1], 4 * py + ex_, t).start()
+    mark("m_wait_dispatch")
+    wait_for(xsa.at[0:15], rsem.at[5])
+    wait_for(xsb.at[0:15], rsem.at[15])
+
+    def to_z(p):
+        for ref, i, k in ((xfa, 10, 1), (xfb, 28, 3)):
+            part_ = ref.at[z, :, half(c)]
+            rcopy(part_, part_, ssem.at[i], zsem.at[k, z], e, 2 * p + c).start()
+
+    over_z(to_z)
+    lax.fori_loop(0, 4, dense_stats, 0)
     over_ep(lambda p: rcopy(stsend.at[p // 4], strecv.at[e], ssem.at[12], rsem.at[7], p, t).start())
     r1g[ex_] = dsg[ex_]
     r1u[ey] = dsu[ey]
@@ -360,11 +404,13 @@
                 target = 4 * other + ex_ if sem == 0 else 4 * ey + other
                 rcopy(got.at[other], left.at[mine], ssem.at[25 + sem], gsem.at[2 + sem], target, t).start()
 
-    for d in range(1, NZ):
+    for d in Z_ORDER:
         p = lax.rem(z + NZ - d, NZ)
-        wait_for(xfull.at[p, :, half(c)], zsem.at[1, p])
-        rcopy(xfull.at[p, :, half(c)], xfull.at[p, :, half(c)], ssem.at[13], z2sem.at[1, p], e, mate).start()
-        if d == SECOND_AT:
+        for ref, i, k in ((xfa, 13, 1), (xfb, 29, 3)):
+            part_ = ref.at[p, :, half(c)]
+            wait_for(part_, zsem.at[k, p])
+            rcopy(part_, part_, ssem.at[i], z2sem.at[k, p], e, mate).start()
+        if d == Z_ORDER[SECOND_AT]:
             second_stage()
 
     mark("p_wait_dense")
@@ -381,6 +427,7 @@
     branch = jnp.sum(jnp.where(at, stats[4:5, :], 0.0), axis=1, keepdims=True)
     rstd2 = lax.rsqrt(sumsq * (1.0 / D) + EPS)
     branch_share = jax.nn.sigmoid(branch * rstd2)
+    hidden = [None, None]
     for h in range(2):
         cg = slice(256 * h, 256 * h + 256)
         g_ = r2g[0, :, cg].astype(F32)
@@ -390,21 +437,32 @@
             u_ = u_ + r2u[i, :, cg].astype(F32)
         g_ = g_ * rstd2
         u_ = u_ * rstd2
-        hall[e, :, cg] = (g_ * jax.nn.sigmoid(g_) * u_ * branch_share).astype(BF16)
-    over_ep(lambda p: rcopy(hall.at[e], hall.at[e], ssem.at[14], rsem.at[8], p, t).start())
+        hidden[h] = (g_ * jax.nn.sigmoid(g_) * u_ * branch_share).astype(BF16)
+    halla[ey, ex_] = hidden[0]
+    hallb[ex_, ey] = hidden[1]
+    for d in (2, 1, 3):
+        px, py = lax.rem(ex_ + d, 4), lax.rem(ey + d, 4)
+        rcopy(halla.at[ey, ex_], halla.at[ey, ex_], ssem.at[14], lsem.at[0], 4 * ey + px, t).start()
+        rcopy(hallb.at[ex_, ey], hallb.at[ex_, ey], ssem.at[30], lsem.at[1], 4 * py + ex_, t).start()
 
     mark("r_wait_expert")
     for i in (20, 21, 22):
         copies[i].wait()
-    for d in range(1, NZ):
+    for d in Z_ORDER:
         p = lax.rem(z + NZ - d, NZ)
-        wait_for(xfull.at[p, :, half(1 - c)], z2sem.at[1, p])
+        wait_for(xfa.at[p, :, half(1 - c)], z2sem.at[1, p])
+        wait_for(xfb.at[p, :, half(1 - c)], z2sem.at[3, p])
 
     mark("s_expert")
     def expert_rows(k, carry):
         tot = jnp.zeros((16, 128), F32)
+
+        def rows_of(cut):
+            third = xfb[k, :, cut].astype(F32)
+            return jnp.concatenate([xfa[k, :, cut].astype(F32), third, jnp.zeros_like(third)], axis=0)
+
         for m in range(4):
-            wide = xfull[k, :, 1024 * m:1024 * m + 1024].astype(F32)
+            wide = rows_of(slice(1024 * m, 1024 * m + 1024))
             sq = wide * wide
             for n in range(8):
                 tot = tot + sq[:, 128 * n:128 * n + 128]
@@ -412,7 +470,7 @@
         rows = pl.ds(pl.multiple_of(k * 16, 16), 16)
         for m in range(4):
             cut = slice(1024 * m, 1024 * m + 1024)
-            aexp[rows, cut] = (xfull[k, :, cut].astype(F32) * scale * gffn[:, cut]).astype(BF16)
+            aexp[rows, cut] = (rows_of(cut) * scale * gffn[:, cut]).astype(BF16)
         return carry
 
     lax.fori_loop(0, NZ, expert_rows, 0)
@@ -430,31 +488,31 @@
     hid = (g_ * jax.nn.sigmoid(g_) * acc[:, 256:512]).astype(BF16)
     aexp[:, 0:256] = hid
 
-    def expert_out(k, carry):
-        cut = pl.ds(pl.multiple_of(k * 512, 512), 512)
-        prod = dot(aexp[:, 0:256], ed[:, cut]).astype(BF16)
+    mark("s3_hidden_stage")
+    wait_for(halla.at[0, 0:3], lsem.at[0])
+    wait_for(hallb.at[0, 0:3], lsem.at[1])
+    for d in (2, 1, 3):
+        px, py = lax.rem(ex_ + d, 4), lax.rem(ey + d, 4)
+        rcopy(halla.at[ey], halla.at[ey], ssem.at[31], lsem.at[2], 4 * py + ex_, t).start()
+        rcopy(hallb.at[ex_], hallb.at[ex_], ssem.at[32], lsem.at[3], 4 * ey + px, t).start()
+    mark("s2_expert_out")
+
+    def chunk_of(k):
+        return lax.rem(k + e, 4)
+
+    def expert_out(part_, k):
+        at_ = pl.ds(pl.multiple_of(part_ * HALF + k * 512, 512), 512)
+        return dot(aexp[:, 0:256], ed[:, at_])
+
+    def for_mate(i, carry):
+        k = chunk_of(i)
+        prod = expert_out(1 - c, k).astype(BF16)
         for n in range(NZ):
-            yp[n, :, cut] = prod[16 * n:16 * n + 16]
-        return carry
-
-    lax.fori_loop(4 * (1 - c), 4 * (1 - c) + 4, expert_out, 0)
-    rcopy(yp.at[:, :, half(1 - c)], yd2d, ssem.at[15], rsem.at[9], e, mate).start()
-    lax.fori_loop(4 * c, 4 * c + 4, expert_out, 0)
-
-    mark("r2_pair_sum")
-    wait_for(yd2d, rsem.at[9])
-
-    def sum_pair(k, carry):
-        both_sum = yp[k, :, half(c)].astype(F32) + yd2d[k].astype(F32)
-        ys[0, k] = both_sum[0:8].astype(BF16)
-        ys[1, k] = both_sum[8:16].astype(BF16)
-        return carry
-
-    lax.fori_loop(0, NZ, sum_pair, 0)
-
-    def back(d, carry):
-        j = lax.rem(d + e, NZ)
-        pe = c * NZ + j
+            yp[k, n] = prod[16 * n:16 * n + 16]
+        rcopy(yp.at[k], yd2d.at[k], ssem.at[15], dsem.at[k], e, mate).start()
+        return carry
+
+    def back(j, pe):
         rcopy(ys.at[1 - c, :, :, cols(j)], yin.at[:, e], ssem.at[18], rsem.at[12], pe, mate).start()
 
         @pl.when(pe != e)
@@ -465,18 +523,32 @@
         def _():
             yin[:, e] = ys[c, :, :, cols(j)]
 
-        return carry
-
-    lax.fori_loop(0, NZ, back, 0)
+    def for_own(i, carry):
+        k = chunk_of(i)
+        prod = expert_out(c, k)
+        at_ = pl.ds(pl.multiple_of(k * 512, 512), 512)
+        wait_for(yd2d.at[k], dsem.at[k])
+        both_sum = jnp.concatenate([prod[16 * n:16 * n + 16] + yd2d[k, n].astype(F32) for n in range(NZ)], axis=0)
+        compact = dot(keep_rows, both_sum.astype(BF16))
+        for n in range(4):
+            ys[n // 2, n % 2, :, at_] = compact[24 * n:24 * n + 24].astype(BF16)
+        for j in range(2):
+            back(2 * k + j, c * NZ + 2 * k + j)
+        return carry
+
+    lax.fori_loop(0, 4, for_mate, 0)
+    lax.fori_loop(0, 4, for_own, 0)
 
     mark("t_wait_hidden")
     copies[19].wait()
-    wait_for(hall.at[0:15], rsem.at[8])
+    wait_for(halla.at[0:3], lsem.at[2])
+    wait_for(hallb.at[0:3], lsem.at[3])
     mark("u_down")
 
     def dense_down(g, carry):
-        block = jnp.concatenate([hall[4 * g + j] for j in range(4)], axis=0)
-        prod = dot(block, dd[...])
+        left = jnp.concatenate([halla[g, j] for j in range(4)], axis=0)
+        right = jnp.concatenate([hallb[j, g] for j in range(4)], axis=0)
+        prod = dot(jnp.concatenate([left, right], axis=1), dd[...])
         for j in range(4):
             part2[2 * g + j // 2, j % 2] = prod[32 * j:32 * j + 32].astype(BF16)
         return carry
@@ -488,13 +560,13 @@
     wait_for(pd2d2, rsem.at[10])
     mark("w_combine")
 
-    def combine(k, carry):
-        rows = yin[k].astype(F32).reshape(128, COLS).astype(BF16)
-        tot = dot(wtab[k, 0], rows) + dot(wtab[k, 1], rows)
-        rsend2[k] = (tot + part2[k, c].astype(F32) + pd2d2[k].astype(F32)).astype(BF16)
-        return carry
-
-    lax.fori_loop(0, NZ, combine, 0)
+    for g in range(2):
+        rows = yin[g].astype(F32).reshape(384, COLS).astype(BF16)
+        tot = dot(wtab[g, 0], rows) + dot(wtab[g, 1], rows)
+        for m in range(4):
+            k = 4 * g + m
+            total_ = tot[32 * m:32 * m + 32] + part2[k, c].astype(F32) + pd2d2[k].astype(F32)
+            rsend2[k] = total_.astype(BF16)
     over_z(lambda p: rcopy(rsend2.at[p], rrecv2.at[z], ssem.at[17], rsem.at[11], e, 2 * p + c).start())
     rrecv2[z] = rsend2[z]
     mark("x_wait_rs")
@@ -505,16 +577,15 @@
     outv[...] = tot.astype(BF16)
 
     mark("z_deliver")
-    def deliver(d, carry):
+    def deliver(d):
         p = lax.rem(z + d, NZ)
 
         @pl.when(jnp.logical_or(t != e, p != z))
         def _():
             rcopy(outv, ofull.at[e], ssem.at[20], osem.at[e], t, 2 * p + c).start()
 
-        return carry
-
-    lax.fori_loop(0, NZ, deliver, 0)
+    for d in Z_ORDER + (0,):
+        deliver(d)
 
     @pl.when(t == e)
     def _():
@@ -553,14 +624,18 @@
     wait_for(wpall.at[0:7 * HD], ssem.at[5])
     wait_for(resall.at[0, 0], ssem.at[6])
     wait_for(rsend2.at[0:7], ssem.at[7])
-    wait_for(xs.at[0:15], ssem.at[8])
+    wait_for(xsa.at[0:15], ssem.at[8])
+    wait_for(xsb.at[0:15], ssem.at[27])
     wait_for(rsend2.at[0:7], ssem.at[9])
-    wait_for(yd2d.at[0:7], ssem.at[10])
+    wait_for(xfa.at[0:7, :, 0:HALF], ssem.at[10])
+    wait_for(xfb.at[0:7, :, 0:HALF], ssem.at[28])
     for i, ref in ((11, dsg), (24, dsu), (25, d2g), (26, d2u)):
         wait_for(ref.at[0:3], ssem.at[i])
     wait_for(strecv.at[0:15], ssem.at[12])
-    wait_for(yd2d.at[0:7], ssem.at[13])
-    wait_for(hall.at[0:15], ssem.at[14])
+    wait_for(xfa.at[0:7, :, 0:HALF], ssem.at[13])
+    wait_for(xfb.at[0:7, :, 0:HALF], ssem.at[29])
+    for i, ref in ((14, halla.at[0]), (30, hallb.at[0]), (31, halla), (32, hallb)):
+        wait_for(ref.at[0:3], ssem.at[i])
     wait_for(yd2d, ssem.at[15])
     wait_for(pd2d2, ssem.at[16])
     wait_for(rsend2.at[0:7], ssem.at[17])
@@ -601,22 +676,23 @@
         vm((D, COLS), BF16), vm((D, COLS), BF16), vm((COLS, D), BF16), vm((COLS, 1024), BF16), vm((512, COLS), BF16),
         vm((N, ROWS, COLS), BF16), vm((N, ROWS, 512), BF16), vm((N, ROWS, 512), BF16), vm((N, ROWS, HD), BF16),
         vm((ROWS, HALF), BF16), vm((ROWS, HD), F32),
-        vm((HALF, COLS), BF16), vm((NZ, 2, ROWS, HD), BF16), vm((NZ, 2, ROWS, COLS), BF16),
+        vm((HALF, COLS), BF16), vm((2, 2, 128, 384), BF16), vm((NZ, 2, ROWS, COLS), BF16),
         vm((NZ, 2, ROWS, COLS), BF16), vm((NZ, ROWS, COLS), BF16), vm((NZ, ROWS, COLS), BF16),
         vm((NZ, ROWS, COLS), BF16),
         vm((8, 128), F32), vm((N, 8, 128), F32),
         vm((4, 4, ROWS, 512), BF16), vm((4, 4, ROWS, 512), BF16), vm((4, 4, ROWS, 512), BF16),
         vm((4, 4, ROWS, 512), BF16), vm((4, ROWS, 512), BF16), vm((4, ROWS, 512), BF16), vm((4, ROWS, 512), BF16),
         vm((4, ROWS, 512), BF16),
-        vm((4, 8, 128), F32), vm((N, 8, 128), F32), vm((N, ROWS, 512), BF16), vm((512, COLS), BF16),
+        vm((4, 8, 128), F32), vm((N, 8, 128), F32), vm((4, 4, ROWS, COLS), BF16),
+        vm((4, 4, ROWS, COLS), BF16), vm((512, COLS), BF16),
         vm((512, COLS), BF16),
-        vm((N, 16, COLS), BF16), vm((NZ, 16, D), BF16), vm((128, D), BF16), vm((128, 512), F32),
-        vm((NZ, 16, D), BF16), vm((NZ, 16, HALF), BF16), vm((2, NZ, 8, HALF), BF16), vm((NZ, N, 8, COLS), BF16),
+        vm((N, 8, COLS), BF16), vm((N, 4, COLS), BF16), vm((NZ, 8, D), BF16), vm((NZ, 4, D), BF16), vm((128, D), BF16), vm((128, 512), F32),
+        vm((4, NZ, 16, 512), BF16), vm((4, NZ, 16, 512), BF16), vm((2, 2, 24, HALF), BF16), vm((2, N, 24, COLS), BF16),
         vm((ROWS, COLS), BF16), vm((N, ROWS, COLS), BF16), vm((ROWS, HD), F32), vm((1, ROWS), F32),
-        pltpu.SemaphoreType.DMA((23,)), pltpu.SemaphoreType.DMA((27,)), pltpu.SemaphoreType.DMA((N,)),
-        pltpu.SemaphoreType.DMA((15,)), pltpu.SemaphoreType.DMA((3, NZ)), pltpu.SemaphoreType.DMA((3, NZ)),
+        pltpu.SemaphoreType.DMA((23,)), pltpu.SemaphoreType.DMA((33,)), pltpu.SemaphoreType.DMA((N,)),
+        pltpu.SemaphoreType.DMA((16,)), pltpu.SemaphoreType.DMA((4, NZ)), pltpu.SemaphoreType.DMA((4, NZ)),
         pltpu.SemaphoreType.DMA((N,)), pltpu.SemaphoreType.DMA((N,)), pltpu.SemaphoreType.DMA((4,)),
-        pltpu.SemaphoreType.DMA((4,)),
+        pltpu.SemaphoreType.DMA((4,)), pltpu.SemaphoreType.DMA((4,)), pltpu.SemaphoreType.DMA((4,)),
     ]
     shapes = (
         jax.ShapeDtypeStruct((ROWS, D), BF16),

time: 95.1 us -> 87.7 us (0.922)
  Pallas kernels: 94.4 us -> 86.5 us
    pallas_call x1, Pallas kernels: 91.8 us -> 83.9 us  [on_device(): pl.pallas_call(layer_kernel, out_shape=shapes, in_specs=[any_] * 23, out_...]
where the time goes in v3:
time: 87.7 us; the launch traced here: 87.1 us
  Pallas kernels  86.5 us (99%)
    pallas_call x1, Pallas kernels, on_device(): pl.pallas_call(layer_kernel, out_shape=shapes, in_specs=[any_] * 23, out_...  83.9 us
    pallas_call x1, Pallas kernels, on_device(): pl.pallas_call(finish_kernel, out_shape=shapes, in_specs=[any_] * 4, out_...  2.56 us

profile of v3, /device:TPU:17, one launch (start us, length us, event | category | flops | bytes accessed | tf_op | source)
XLA Modules:
  0.0 87.1 jit_solution(1312641742741566809)
XLA Ops:
  0.6 83.9 %layer.1 = (bf16[32,4096]{1,0:T(8,128)(2,1)}, f32[32,128,128]{2,1,0:T(8,128)}, f32[32,128]{1,0:T(8,128)}, f32[1,32]{1,0:T(1,128)}) custom-call(bf16[32,4096]{1,0:T(8,128)(2,1)} %tok_h.1, f32[32,128,128]{2,1,0:T(8,128)} %bitcast.18, f32[32,128]{1,0:T(8,128)} %bitcast.21, f32[1,32]{1,0:T(1,128)} %bitcast.27, f32[1,4096]{1,0:T(1,128)} %bitcast.22, ...), custom_call_target="tpu_custom_call" | custom-call | tf_op jit(solution)/shard_map/layer/pallas_call | solution.py:703
  84.6 2.6 %finish.1 = (bf16[32,4096]{1,0:T(8,128)(2,1)}, f32[32,128,128]{2,1,0:T(8,128)}, f32[32,128]{1,0:T(8,128)}, f32[1,32]{1,0:T(1,128)}) custom-call(bf16[32,4096]{1,0:T(8,128)(2,1)} %get-tuple-element.12.out_a, f32[32,128,128]{2,1,0:T(8,128)} %get-tuple-element.13.nm_a, f32[32,128]{1,0:T(8,128)} %get-tuple-element.14.nn_a, f32[1,32]{1,0:T(1,128)} %get-tuple-element.15.nmax_a), custom_call_target="tpu_custom_call" | custom-call | tf_op jit(solution)/shard_map/finish/pallas_call | solution.py:719

commit v4 on v3

--- a/solution.py
+++ b/solution.py
@@ -18,7 +18,7 @@
 COLS = 256
 HALF = 2048
 HD = 128
-SECOND_AT = 1
+SECOND_AT = 0
 HOPS = (0, 1, 2, 1)
 EP_ORDER = sorted(
     [(dy, dx) for dy in range(4) for dx in range(4) if dy + dx], key=lambda o: -(HOPS[o[0]] + HOPS[o[1]])
@@ -37,14 +37,14 @@
 def layer_kernel(
     tok_h, st_h, sn_h, smax_h, gmix_h, wq_h, wk_h, wv_h, wo_h, wi_h, wf_h, fb_h, wp_h, gffn_h, wbr_h,
     rt_h, rw_h, eg_h, eu_h, ed_h, dg_h, du_h, dd_h,
-    out_h, nm_h, nn_h, nmax_h,
+    ofull, nm, nnv, nmaxv,
     tok, st, sn, smax, gmix, wq, wi, wf, fb, wp, gffn, wbr, rt, rw, eg, eu, ed, dgu, dd,
     xall, csend, crecv, mhall, heads, num,
     wpall, wtab, resall,
     part2, pd2d2, rsend2, rrecv2,
     rtsend, rtall, dsg, dsu, r1g, r1u, d2g, d2u, r2g, r2u, stsend, strecv, halla, hallb, r2all, aall,
-    xsa, xsb, xfa, xfb, aexp, acc, yp, yd2d, ys, yin, outv, ofull, nnv, nmaxv,
-    load_sem, ssem, bsem, rsem, zsem, z2sem, osem, hsem, gsem, dsem, lsem, store_sem,
+    xsa, xsb, xfa, xfb, aexp, acc, yp, yd2d, ys, yin, outv,
+    load_sem, ssem, bsem, rsem, zsem, z2sem, osem, hsem, gsem, dsem, lsem,
 ):
     e = lax.axis_index("ep")
     t = lax.axis_index("tp")
@@ -189,6 +189,9 @@
             else:
                 crecv[e] = piece
     mark("d_wait_qkvo")
+    keep_w = jnp.broadcast_to(keep, (ROWS, HD))
+    for b in range(ROWS):
+        st[b] = keep_w[b:b + 1, :] * st[b]
     wait_for(crecv.at[0:15], rsem.at[1])
     mark("e_cell")
     qkvo = crecv[0].astype(F32)
@@ -198,14 +201,13 @@
     q = qkvo[:, 0:128]
     kw = qkvo[:, 128:256] * (HD ** -0.5) * write
     v = qkvo[:, 256:384]
-    keep_w = jnp.broadcast_to(keep, (ROWS, HD))
     new_norm = keep_w * sn[...] + kw
     nnv[...] = new_norm
     kw_t = jnp.transpose(kw)
     q_t = jnp.transpose(q)
     for b in range(ROWS):
-        new = keep_w[b:b + 1, :] * st[b] + kw_t[:, b:b + 1] * v[b:b + 1, :]
-        st[b] = new
+        new = st[b] + kw_t[:, b:b + 1] * v[b:b + 1, :]
+        nm[b] = new
         num[b:b + 1, :] = jnp.sum(q_t[:, b:b + 1] * new, axis=0, keepdims=True)
     denom = jnp.maximum(jnp.abs(jnp.sum(q * new_norm, axis=1, keepdims=True)), 1.0)
     mhall[e] = (jax.nn.sigmoid(qkvo[:, 384:512]) * (num[...] / denom)).astype(BF16)
@@ -220,14 +222,6 @@
         @pl.when(p == t)
         def _():
             heads[:, head_cols] = mhall[p]
-
-    stores = [
-        pltpu.make_async_copy(st, nm_h, store_sem.at[0]),
-        pltpu.make_async_copy(nnv, nn_h, store_sem.at[1]),
-        pltpu.make_async_copy(nmaxv, nmax_h, store_sem.at[2]),
-    ]
-    for store in stores:
-        store.start()
 
     mark("f_tables")
     wait_for(rtall.at[0:15], rsem.at[0])
@@ -335,32 +329,42 @@
         rcopy(resall.at[p, c], resall.at[p, c], ssem.at[9], z2sem.at[0, p], e, mate).start()
 
     mark("n_wait_fwd_dense")
+    def rows_for(k, par):
+        return pl.ds(pl.multiple_of(64 * k + 32 * par, 32), 32)
+
+    def dense_rows(par):
+        for k in range(NZ):
+            wide = resall[k, par].astype(F32)
+            r2all[rows_for(k, par), :] = (wide * wide).astype(BF16)
+            aall[rows_for(k, par), :] = (wide * gain_f).astype(BF16)
+
+    def dense_part(i, par, upper):
+        lhs = jnp.concatenate([aall[rows_for(4 * i + j, par), :] for j in range(4)], axis=0)
+        prod = dot(lhs, dgu[:, 512:1024] if upper else dgu[:, 0:512])
+        for j in range(4):
+            piece = prod[32 * j:32 * j + 32].astype(BF16)
+            py, px = 2 * i + j // 2, 2 * (j % 2) + par
+            if upper:
+                dsu[py, px] = piece
+            else:
+                dsg[px, py] = piece
+
+    def both_parts(i, carry):
+        dense_part(i, c, True)
+        dense_part(i, c, False)
+        return carry
+
+    dense_rows(c)
+    lax.fori_loop(0, 2, both_parts, 0)
     for d in Z_ORDER:
         p = lax.rem(z + NZ - d, NZ)
         wait_for(resall.at[p, 1 - c], z2sem.at[0, p])
-    for k in range(NZ):
-        wide = jnp.concatenate([resall[k, 0], resall[k, 1]], axis=0).astype(F32)
-        r2all[64 * k:64 * k + 64] = (wide * wide).astype(BF16)
-        aall[64 * k:64 * k + 64] = (wide * gain_f).astype(BF16)
-    def dense_up(i, carry):
-        g = lax.rem(ey + 1 + i, 4)
-        rows = pl.ds(pl.multiple_of(g * 128, 128), 128)
-        prod = dot(aall[rows, :], dgu[:, 512:1024])
-        for j in range(4):
-            dsu[g, j] = prod[32 * j:32 * j + 32].astype(BF16)
-
-        @pl.when(g != ey)
-        def _():
-            rcopy(dsu.at[g], r1u.at[ey], ssem.at[24], gsem.at[1], 4 * g + ex_, t).start()
-
-        return carry
-
-    def dense_gate(g, carry):
-        rows = pl.ds(pl.multiple_of(g * 128, 128), 128)
-        prod = dot(aall[rows, :], dgu[:, 0:512])
-        for j in range(4):
-            dsg[j, g] = prod[32 * j:32 * j + 32].astype(BF16)
-        return carry
+    dense_rows(1 - c)
+    lax.fori_loop(0, 2, lambda i, carry: (dense_part(i, 1 - c, True), carry)[1], 0)
+    for d in (2, 1, 3):
+        py = lax.rem(ey + d, 4)
+        rcopy(dsu.at[py], r1u.at[ey], ssem.at[24], gsem.at[1], 4 * py + ex_, t).start()
+    lax.fori_loop(0, 2, lambda i, carry: (dense_part(i, 1 - c, False), carry)[1], 0)
 
     def dense_stats(g, carry):
         rows = pl.ds(pl.multiple_of(g * 128, 128), 128)
@@ -370,8 +374,6 @@
         stsend[g] = jnp.where(sub8 < 4, stat, br)
         return carry
 
-    lax.fori_loop(0, 4, dense_up, 0)
-    lax.fori_loop(0, 4, dense_gate, 0)
     for d in (2, 1, 3):
         px = lax.rem(ex_ + d, 4)
         rcopy(dsg.at[px], r1g.at[ex_], ssem.at[11], gsem.at[0], 4 * ey + px, t).start()
@@ -453,7 +455,7 @@
         wait_for(xfa.at[p, :, half(1 - c)], z2sem.at[1, p])
         wait_for(xfb.at[p, :, half(1 - c)], z2sem.at[3, p])
 
-    mark("s_expert")
+    mark("r2_rows")
     def expert_rows(k, carry):
         tot = jnp.zeros((16, 128), F32)
 
@@ -474,6 +476,7 @@
         return carry
 
     lax.fori_loop(0, NZ, expert_rows, 0)
+    mark("s_expert")
     acc[...] = jnp.zeros_like(acc)
 
     def expert_in(k, carry):
@@ -582,14 +585,14 @@
 
         @pl.when(jnp.logical_or(t != e, p != z))
         def _():
-            rcopy(outv, ofull.at[e], ssem.at[20], osem.at[e], t, 2 * p + c).start()
+            rcopy(outv, ofull.at[:, cols(e)], ssem.at[20], osem.at[e], t, 2 * p + c).start()
 
     for d in Z_ORDER + (0,):
         deliver(d)
 
     @pl.when(t == e)
     def _():
-        ofull[e] = outv[...]
+        ofull[:, cols(e)] = outv[...]
 
     first = c == lax.rem(e, 2)
 
@@ -600,19 +603,17 @@
 
             @pl.when(jnp.logical_or(t != e, p != e))
             def _():
-                wait_for(ofull.at[p], osem.at[p])
-
-            rcopy(ofull.at[p], out_h.at[:, cols(p)], ssem.at[22], rsem.at[14], e, mate).start()
-            pltpu.make_async_copy(ofull.at[p], out_h.at[:, cols(p)], store_sem.at[3]).start()
+                wait_for(ofull.at[:, cols(p)], osem.at[p])
+
+            rcopy(ofull.at[:, cols(p)], ofull.at[:, cols(p)], ssem.at[22], rsem.at[14], e, mate).start()
             return carry
 
         lax.fori_loop(0, N, pass_on, 0)
-        wait_for(ofull, store_sem.at[3])
         wait_for(ofull, ssem.at[22])
 
     @pl.when(jnp.logical_not(first))
     def _():
-        wait_for(out_h, rsem.at[14])
+        wait_for(ofull, rsem.at[14])
 
     mark("zz_end")
     wait_for(xall.at[0:15], ssem.at[0])
@@ -643,23 +644,17 @@
     either(e // NZ == c, yin.at[:, 0:7], yin.at[:, 0:8], ssem.at[19])
     either(t == e, rsend2.at[0:7], rsend2, ssem.at[20])
     wait_for(wpall.at[0:7 * HD], ssem.at[21])
-    for store in stores:
-        store.wait()
     mark(None)
 
 
-def finish_kernel(out_a, nm_a, nn_a, nmax_a, out_o, nm_o, nn_o, nmax_o, out_v, nm_v, nn_v, nmax_v, in_sem, out_sem):
-    trips = [(nm_a.at[8 * k:8 * k + 8], nm_v.at[8 * k:8 * k + 8], nm_o.at[8 * k:8 * k + 8]) for k in range(4)]
-    trips += [(out_a, out_v, out_o), (nn_a, nn_v, nn_o), (nmax_a, nmax_v, nmax_o)]
-    ins = [pltpu.make_async_copy(a, v, in_sem.at[i]) for i, (a, v, _) in enumerate(trips)]
-    outs = [pltpu.make_async_copy(v, o, out_sem.at[i]) for i, (_, v, o) in enumerate(trips)]
-    for copy in ins:
+def finish_kernel(out_v, nm_v, nn_v, nmax_v, out_o, nm_o, nn_o, nmax_o, sem):
+    trips = [(nm_v.at[8 * k:8 * k + 8], nm_o.at[8 * k:8 * k + 8]) for k in range(4)]
+    trips += [(out_v, out_o), (nn_v, nn_o), (nmax_v, nmax_o)]
+    copies = [pltpu.make_async_copy(a, b, sem.at[i]) for i, (a, b) in enumerate(trips)]
+    for copy in copies:
         copy.start()
-    for got, put in zip(ins, outs):
-        got.wait()
-        put.start()
-    for put in outs:
-        put.wait()
+    for copy in copies:
+        copy.wait()
 
 
 def on_device(
@@ -667,7 +662,8 @@
     forget_bias, w_proj, ffn_gain, w_branch, routes, route_weight, expert_gate, expert_up, expert_down,
     dense_gate, dense_up, dense_down,
 ):
-    any_ = pl.BlockSpec(memory_space=pl.ANY)
+    any_ = pl.BlockSpec(memory_space=pltpu.HBM)
+    local = pl.BlockSpec(memory_space=pltpu.VMEM)
     vm = pltpu.VMEM
     scratch = [
         vm((ROWS, D), BF16), vm((ROWS, HD, HD), F32), vm((ROWS, HD), F32), vm((1, ROWS), F32), vm((1, D), F32),
@@ -688,23 +684,17 @@
         vm((512, COLS), BF16),
         vm((N, 8, COLS), BF16), vm((N, 4, COLS), BF16), vm((NZ, 8, D), BF16), vm((NZ, 4, D), BF16), vm((128, D), BF16), vm((128, 512), F32),
         vm((4, NZ, 16, 512), BF16), vm((4, NZ, 16, 512), BF16), vm((2, 2, 24, HALF), BF16), vm((2, N, 24, COLS), BF16),
-        vm((ROWS, COLS), BF16), vm((N, ROWS, COLS), BF16), vm((ROWS, HD), F32), vm((1, ROWS), F32),
+        vm((ROWS, COLS), BF16),
         pltpu.SemaphoreType.DMA((23,)), pltpu.SemaphoreType.DMA((33,)), pltpu.SemaphoreType.DMA((N,)),
         pltpu.SemaphoreType.DMA((16,)), pltpu.SemaphoreType.DMA((4, NZ)), pltpu.SemaphoreType.DMA((4, NZ)),
         pltpu.SemaphoreType.DMA((N,)), pltpu.SemaphoreType.DMA((N,)), pltpu.SemaphoreType.DMA((4,)),
-        pltpu.SemaphoreType.DMA((4,)), pltpu.SemaphoreType.DMA((4,)), pltpu.SemaphoreType.DMA((4,)),
+        pltpu.SemaphoreType.DMA((4,)), pltpu.SemaphoreType.DMA((4,)),
     ]
-    shapes = (
-        jax.ShapeDtypeStruct((ROWS, D), BF16),
-        jax.ShapeDtypeStruct((ROWS, HD, HD), F32),
-        jax.ShapeDtypeStruct((ROWS, HD), F32),
-        jax.ShapeDtypeStruct((1, ROWS), F32),
-    )
     results = pl.pallas_call(
         layer_kernel,
-        out_shape=shapes,
+        out_shape=(vm((ROWS, D), BF16), vm((ROWS, HD, HD), F32), vm((ROWS, HD), F32), vm((1, ROWS), F32)),
         in_specs=[any_] * 23,
-        out_specs=(any_,) * 4,
+        out_specs=(local,) * 4,
         scratch_shapes=scratch,
         compiler_params=pltpu.CompilerParams(
             collective_id=0, has_side_effects=True, vmem_limit_bytes=60 * 1024 * 1024
@@ -718,11 +708,14 @@
     )
     out, nm, nn, nmax = pl.pallas_call(
         finish_kernel,
-        out_shape=shapes,
-        in_specs=[any_] * 4,
+        out_shape=(
+            jax.ShapeDtypeStruct((ROWS, D), BF16), jax.ShapeDtypeStruct((ROWS, HD, HD), F32),
+            jax.ShapeDtypeStruct((ROWS, HD), F32), jax.ShapeDtypeStruct((1, ROWS), F32),
+        ),
+        in_specs=[local] * 4,
         out_specs=(any_,) * 4,
-        scratch_shapes=[vm(shape.shape, shape.dtype) for shape in shapes]
-        + [pltpu.SemaphoreType.DMA((7,)), pltpu.SemaphoreType.DMA((7,))],
+        scratch_shapes=[pltpu.SemaphoreType.DMA((7,))],
+        compiler_params=pltpu.CompilerParams(vmem_limit_bytes=8 * 1024 * 1024),
         name="finish",
     )(*results)
     return (

time: 87.7 us -> 85.4 us (0.974)
  Pallas kernels: 86.5 us -> 84 us
    pallas_call x2, Pallas kernels: 86.5 us -> 84 us  [the longest x1 82.6 us: on_device(): pl.pallas_call(layer_kernel, out_shape=(vm((ROWS, D), BF16), vm((ROWS, HD...]
where the time goes in v4:
time: 85.4 us; the launch traced here: 84.7 us
  Pallas kernels  84 us (98%)
    pallas_call x1, Pallas kernels, on_device(): pl.pallas_call(layer_kernel, out_shape=(vm((ROWS, D), BF16), vm((ROWS, HD...  82.6 us

profile of v4, /device:TPU:17, one launch (start us, length us, event | category | flops | bytes accessed | tf_op | source)
XLA Modules:
  0.0 84.7 jit_solution(515757965641203574)
XLA Ops:
  0.6 82.6 %layer.1 = (bf16[32,4096]{1,0:T(8,128)(2,1)S(1)}, f32[32,128,128]{2,1,0:T(8,128)S(1)}, f32[32,128]{1,0:T(8,128)S(1)}, f32[1,32]{1,0:T(1,128)S(1)}) custom-call(bf16[32,4096]{1,0:T(8,128)(2,1)} %tok_h.1, f32[32,128,128]{2,1,0:T(8,128)} %bitcast.18, f32[32,128]{1,0:T(8,128)} %bitcast.21, f32[1,32]{1,0:T(1,128)} %bitcast.27, f32[1,4096]{1,0:T(1,128)} %bitcast.22, ...), custom_call_target="tpu_custom_call" | custom-call | tf_op jit(solution)/shard_map/layer/pallas_call | solution.py:693
  83.2 1.5 %finish.1 = (bf16[32,4096]{1,0:T(8,128)(2,1)}, f32[32,128,128]{2,1,0:T(8,128)}, f32[32,128]{1,0:T(8,128)}, f32[1,32]{1,0:T(1,128)}) custom-call(bf16[32,4096]{1,0:T(8,128)(2,1)S(1)} %get-tuple-element.12.out_v, f32[32,128,128]{2,1,0:T(8,128)S(1)} %get-tuple-element.13.nm_v, f32[32,128]{1,0:T(8,128)S(1)} %get-tuple-element.14.nn_v, ...), custom_call_target="tpu_custom_call" | custom-call | tf_op jit(solution)/shard_map/finish/pallas_call | solution.py:709

commit v5 on v4

--- a/solution.py
+++ b/solution.py
@@ -42,7 +42,7 @@
     xall, csend, crecv, mhall, heads, num,
     wpall, wtab, resall,
     part2, pd2d2, rsend2, rrecv2,
-    rtsend, rtall, dsg, dsu, r1g, r1u, d2g, d2u, r2g, r2u, stsend, strecv, halla, hallb, r2all, aall,
+    rtsend, rtall, dsg, dsu, r1g, r1u, d2g, d2u, r2g, r2u, stsend, strecv, halla, hallb, hallc, r2all, aall,
     xsa, xsb, xfa, xfb, aexp, acc, yp, yd2d, ys, yin, outv,
     load_sem, ssem, bsem, rsem, zsem, z2sem, osem, hsem, gsem, dsem, lsem,
 ):
@@ -203,15 +203,16 @@
     v = qkvo[:, 256:384]
     new_norm = keep_w * sn[...] + kw
     nnv[...] = new_norm
-    kw_t = jnp.transpose(kw)
     q_t = jnp.transpose(q)
     for b in range(ROWS):
-        new = st[b] + kw_t[:, b:b + 1] * v[b:b + 1, :]
-        nm[b] = new
-        num[b:b + 1, :] = jnp.sum(q_t[:, b:b + 1] * new, axis=0, keepdims=True)
+        num[b:b + 1, :] = jnp.sum(q_t[:, b:b + 1] * st[b], axis=0, keepdims=True)
+    numer = num[...] + jnp.sum(q * kw, axis=1, keepdims=True) * v
     denom = jnp.maximum(jnp.abs(jnp.sum(q * new_norm, axis=1, keepdims=True)), 1.0)
-    mhall[e] = (jax.nn.sigmoid(qkvo[:, 384:512]) * (num[...] / denom)).astype(BF16)
+    mhall[e] = (jax.nn.sigmoid(qkvo[:, 384:512]) * (numer / denom)).astype(BF16)
     over_ep(lambda p: rcopy(mhall.at[e], mhall.at[e], ssem.at[23], hsem.at[e], p, t).start())
+    kw_t = jnp.transpose(kw)
+    for b in range(ROWS):
+        nm[b] = st[b] + kw_t[:, b:b + 1] * v[b:b + 1, :]
     head_cols = pl.ds(pl.multiple_of(t * HD, HD), HD)
 
     def turn_heads(p):
@@ -262,11 +263,15 @@
         p = lax.rem(z + NZ - d, NZ)
         wait_for(wp_rows(2 * p + c), zsem.at[2, p])
         rcopy(wp_rows(2 * p + c), wp_rows(2 * p + c), ssem.at[21], z2sem.at[2, p], e, mate).start()
-    turn_heads(e)
-    for offset in EP_ORDER:
-        p = behind(offset)
-        wait_for(mhall.at[p], hsem.at[p])
-        turn_heads(p)
+    for d in Z_ORDER + (0,):
+        for k in range(2):
+            p = 2 * lax.rem(z + d, NZ) + k
+
+            @pl.when(p != e)
+            def _(p=p):
+                wait_for(mhall.at[p], hsem.at[p])
+
+            turn_heads(p)
     mark("g_wait_heads")
     def combine_table(k, carry):
         turned = jnp.transpose(table(2 * k + c))[0:ROWS, :]
@@ -440,12 +445,14 @@
         g_ = g_ * rstd2
         u_ = u_ * rstd2
         hidden[h] = (g_ * jax.nn.sigmoid(g_) * u_ * branch_share).astype(BF16)
-    halla[ey, ex_] = hidden[0]
-    hallb[ex_, ey] = hidden[1]
+    halla[ey, ex_] = hidden[1][:, 0:128]
+    hallb[ex_, ey] = hidden[1][:, 128:256]
+    hallc[e] = hidden[0]
     for d in (2, 1, 3):
         px, py = lax.rem(ex_ + d, 4), lax.rem(ey + d, 4)
         rcopy(halla.at[ey, ex_], halla.at[ey, ex_], ssem.at[14], lsem.at[0], 4 * ey + px, t).start()
         rcopy(hallb.at[ex_, ey], hallb.at[ex_, ey], ssem.at[30], lsem.at[1], 4 * py + ex_, t).start()
+    over_ep(lambda p: rcopy(hallc.at[e], hallc.at[e], ssem.at[33], rsem.at[8], p, t).start())
 
     mark("r_wait_expert")
     for i in (20, 21, 22):
@@ -546,12 +553,16 @@
     copies[19].wait()
     wait_for(halla.at[0:3], lsem.at[2])
     wait_for(hallb.at[0:3], lsem.at[3])
+    wait_for(hallc.at[0:15], rsem.at[8])
     mark("u_down")
 
     def dense_down(g, carry):
-        left = jnp.concatenate([halla[g, j] for j in range(4)], axis=0)
-        right = jnp.concatenate([hallb[j, g] for j in range(4)], axis=0)
-        prod = dot(jnp.concatenate([left, right], axis=1), dd[...])
+        parts = (
+            jnp.concatenate([hallc[4 * g + j] for j in range(4)], axis=0),
+            jnp.concatenate([halla[g, j] for j in range(4)], axis=0),
+            jnp.concatenate([hallb[j, g] for j in range(4)], axis=0),
+        )
+        prod = dot(jnp.concatenate(parts, axis=1), dd[...])
         for j in range(4):
             part2[2 * g + j // 2, j % 2] = prod[32 * j:32 * j + 32].astype(BF16)
         return carry
@@ -598,17 +609,16 @@
 
     @pl.when(first)
     def _():
-        def pass_on(d, carry):
-            p = down(d)
-
+        def pass_on(p):
             @pl.when(jnp.logical_or(t != e, p != e))
             def _():
                 wait_for(ofull.at[:, cols(p)], osem.at[p])
 
             rcopy(ofull.at[:, cols(p)], ofull.at[:, cols(p)], ssem.at[22], rsem.at[14], e, mate).start()
-            return carry
-
-        lax.fori_loop(0, N, pass_on, 0)
+
+        pass_on(e)
+        for offset in EP_ORDER[::-1]:
+            pass_on(behind(offset))
         wait_for(ofull, ssem.at[22])
 
     @pl.when(jnp.logical_not(first))
@@ -617,6 +627,7 @@
 
     mark("zz_end")
     wait_for(xall.at[0:15], ssem.at[0])
+    wait_for(hallc.at[0:15], ssem.at[33])
     wait_for(rtall.at[0:15], ssem.at[1])
     wait_for(csend.at[0:15], ssem.at[2])
     wait_for(heads.at[:, 0:15 * HD], ssem.at[3])
@@ -679,13 +690,13 @@
         vm((4, 4, ROWS, 512), BF16), vm((4, 4, ROWS, 512), BF16), vm((4, 4, ROWS, 512), BF16),
         vm((4, 4, ROWS, 512), BF16), vm((4, ROWS, 512), BF16), vm((4, ROWS, 512), BF16), vm((4, ROWS, 512), BF16),
         vm((4, ROWS, 512), BF16),
-        vm((4, 8, 128), F32), vm((N, 8, 128), F32), vm((4, 4, ROWS, COLS), BF16),
-        vm((4, 4, ROWS, COLS), BF16), vm((512, COLS), BF16),
+        vm((4, 8, 128), F32), vm((N, 8, 128), F32), vm((4, 4, ROWS, HD), BF16),
+        vm((4, 4, ROWS, HD), BF16), vm((N, ROWS, COLS), BF16), vm((512, COLS), BF16),
         vm((512, COLS), BF16),
         vm((N, 8, COLS), BF16), vm((N, 4, COLS), BF16), vm((NZ, 8, D), BF16), vm((NZ, 4, D), BF16), vm((128, D), BF16), vm((128, 512), F32),
         vm((4, NZ, 16, 512), BF16), vm((4, NZ, 16, 512), BF16), vm((2, 2, 24, HALF), BF16), vm((2, N, 24, COLS), BF16),
         vm((ROWS, COLS), BF16),
-        pltpu.SemaphoreType.DMA((23,)), pltpu.SemaphoreType.DMA((33,)), pltpu.SemaphoreType.DMA((N,)),
+        pltpu.SemaphoreType.DMA((23,)), pltpu.SemaphoreType.DMA((34,)), pltpu.SemaphoreType.DMA((N,)),
         pltpu.SemaphoreType.DMA((16,)), pltpu.SemaphoreType.DMA((4, NZ)), pltpu.SemaphoreType.DMA((4, NZ)),
         pltpu.SemaphoreType.DMA((N,)), pltpu.SemaphoreType.DMA((N,)), pltpu.SemaphoreType.DMA((4,)),
         pltpu.SemaphoreType.DMA((4,)), pltpu.SemaphoreType.DMA((4,)),

time: 85.4 us -> 84.3 us (0.987)
  no operation moved by 1% of the time
where the time goes in v5:
time: 84.3 us; the launch traced here: 83.9 us
  Pallas kernels  83.2 us (99%)
    pallas_call x1, Pallas kernels, on_device(): pl.pallas_call(layer_kernel, out_shape=(vm((ROWS, D), BF16), vm((ROWS, HD...  81.7 us

profile of v5, /device:TPU:17, one launch (start us, length us, event | category | flops | bytes accessed | tf_op | source)
XLA Modules:
  0.0 83.9 jit_solution(11810427840430621505)
XLA Ops:
  0.6 81.7 %layer.1 = (bf16[32,4096]{1,0:T(8,128)(2,1)S(1)}, f32[32,128,128]{2,1,0:T(8,128)S(1)}, f32[32,128]{1,0:T(8,128)S(1)}, f32[1,32]{1,0:T(1,128)S(1)}) custom-call(bf16[32,4096]{1,0:T(8,128)(2,1)} %tok_h.1, f32[32,128,128]{2,1,0:T(8,128)} %bitcast.18, f32[32,128]{1,0:T(8,128)} %bitcast.21, f32[1,32]{1,0:T(1,128)} %bitcast.27, f32[1,4096]{1,0:T(1,128)} %bitcast.22, ...), custom_call_target="tpu_custom_call" | custom-call | tf_op jit(solution)/shard_map/layer/pallas_call | solution.py:704
  82.4 1.5 %finish.1 = (bf16[32,4096]{1,0:T(8,128)(2,1)}, f32[32,128,128]{2,1,0:T(8,128)}, f32[32,128]{1,0:T(8,128)}, f32[1,32]{1,0:T(1,128)}) custom-call(bf16[32,4096]{1,0:T(8,128)(2,1)S(1)} %get-tuple-element.12.out_v, f32[32,128,128]{2,1,0:T(8,128)S(1)} %get-tuple-element.13.nm_v, f32[32,128]{1,0:T(8,128)S(1)} %get-tuple-element.14.nn_v, ...), custom_call_target="tpu_custom_call" | custom-call | tf_op jit(solution)/shard_map/finish/pallas_call | solution.py:720
